TPU v7x, 32 devices: a whole 2x2x4 slice. The times are simulated.
32 devices in a mesh: grp: 2 (over x), tp: 4 (over y, core), dp: 4 (over z).
Axes of the slice: x: 2, y: 2, z: 4, core: 2. Of those that a mesh axis runs over, the one named last changes fastest.
Arguments:
- tokens: bfloat16 [64, 4096], P(('grp', 'tp'), 'dp'), parts along dimension 0, may hold values from -45 to 45
- w_in: bfloat16 [2, 2, 4096, 8192], P(None, None, 'dp', 'tp'), may hold values from -0.09375 to 0.09375
- w_vec: bfloat16 [2, 2, 4096, 2048], P(None, None, 'dp', 'tp'), may hold values from -0.09375 to 0.09375
- w_step: bfloat16 [2, 4096, 128], P(None, 'dp'), may hold values from -0.09375 to 0.09375
- conv_weight: bfloat16 [2, 4, 8192], P(None, None, 'tp'), may hold values from -3 to 3
- conv_vec: bfloat16 [2, 2, 4, 2048], P(None, None, None, 'tp'), may hold values from -3 to 3
- conv_state: bfloat16 [2, 64, 3, 8192], P(None, ('grp', 'dp'), None, 'tp'), parts along dimension 1, may hold values from -6 to 6
- vec_state: bfloat16 [2, 2, 64, 3, 2048], P(None, None, ('grp', 'dp'), None, 'tp'), parts along dimension 2, may hold values from -6 to 6
- ssm_state: float32 [2, 64, 128, 64, 128], P(None, ('grp', 'dp'), 'tp'), parts along dimension 1, may hold values from -4 to 4
- step_bias: float32 [2, 128], P(None, 'tp'), may hold values from -1.5 to 1
- decay_log: float32 [2, 128], P(None, 'tp'), may hold values from -4 to 1
- skip_gain: float32 [2, 128], P(None, 'tp'), may hold values from 0.5 to 3
- mix_gain: bfloat16 [2, 4096], P(None, 'dp'), may hold values from 0.099609375 to 1.8984375
- out_gain: bfloat16 [2, 8192], P(None, 'tp'), may hold values from 0.099609375 to 1.8984375
- w_out: bfloat16 [2, 8192, 4096], P(None, 'tp', 'dp'), may hold values from -0.0625 to 0.0625
Outputs:
- new_tokens: bfloat16 [64, 4096], P(('grp', 'tp'), 'dp'), parts along dimension 0
- new_conv: bfloat16 [2, 64, 3, 8192], P(None, ('grp', 'dp'), None, 'tp'), parts along dimension 1
- new_vec: bfloat16 [2, 2, 64, 3, 2048], P(None, None, ('grp', 'dp'), None, 'tp'), parts along dimension 2
- new_ssm: float32 [2, 64, 128, 64, 128], P(None, ('grp', 'dp'), 'tp'), parts along dimension 1
There are 2 independent parts, one for each index of `grp`. A program takes and returns all parts, laid end to end along the dimension named above; an argument that names none is the same for every part. Nothing has to cross between parts.
All inputs are finite; a program needn't handle non-finite values.
Results may differ from a plain program's by a relative error of at most 0.023.
Values may be sent and summed in bfloat16 or wider, within the bound.
A program may use at most 128 MiB of HBM per device.

v0:
```python
import functools

import jax
import jax.numpy as jnp
from jax import lax
from jax.experimental import pallas as pl
from jax.experimental.pallas import tpu as pltpu
from jax.sharding import PartitionSpec as P

MODEL_WIDTH = 4096
HEAD_COUNT = 128
HEAD_DIM = 64
STATE_DIM = 128
GROUP_COUNT = 16
LAYER_COUNT = 2

EPS = 1e-06
F32 = jnp.float32
BF16 = jnp.bfloat16


def remote(src, dst, send_sem, recv_sem, axis, target):
    return pltpu.make_async_remote_copy(
        src_ref=src,
        dst_ref=dst,
        send_sem=send_sem,
        recv_sem=recv_sem,
        device_id={axis: target},
        device_id_type=pl.DeviceIdType.MESH,
    )


def greet(sizes):
    barrier = pltpu.get_barrier_semaphore()
    count = 0
    for axis, n in sizes:
        me = lax.axis_index(axis)
        for k in range(1, n):
            pl.semaphore_signal(
                barrier,
                inc=1,
                device_id={axis: lax.rem(me + k, n)},
                device_id_type=pl.DeviceIdType.MESH,
            )
            count += 1
    pl.semaphore_wait(barrier, count)


def spread(src, dst, send_sem, recv_sem, axis, n):
    me = lax.axis_index(axis)
    copies = []
    for k in range(1, n):
        copy = remote(src, dst.at[me], send_sem.at[k], recv_sem.at[k], axis, lax.rem(me + k, n))
        copy.start()
        copies.append(copy)
    return copies


def deal(src, dst, send_sem, recv_sem, axis, n, whole=False):
    me = lax.axis_index(axis)
    copies = []
    for k in range(1, n):
        peer = lax.rem(me + k, n)
        copy = remote(
            src if whole else src.at[peer],
            dst.at[k],
            send_sem.at[k],
            recv_sem.at[k],
            axis,
            peer,
        )
        copy.start()
        copies.append(copy)
    return copies


def project(
    layer, ndp, rows_d, lhs, squares, weights, loads, w_step_ref, send, recv, sems, outs
):
    w_in_buf, w_vec_buf = weights
    load_in, load_vec = loads
    send_gate, send_val, send_small = send
    recv_gate, recv_val, recv_small = recv
    proj_ref, vecs_ref, step_ref = outs
    vec_cols = w_vec_buf.shape[2]
    cols = w_in_buf.shape[2]
    heads = w_step_ref.shape[2]
    me = lax.axis_index("dp")

    def put(target, at, acc):
        for p in range(ndp):
            target[p, :, at : at + acc.shape[1]] = acc[p * rows_d : (p + 1) * rows_d].astype(BF16)

    put(send_small, 2 * vec_cols, jnp.dot(lhs, w_step_ref[layer], preferred_element_type=F32))
    put(send_small, 2 * vec_cols + heads, jnp.broadcast_to(squares, (squares.shape[0], 128)))
    load_vec.wait()
    for role in range(2):
        put(send_small, role * vec_cols, jnp.dot(lhs, w_vec_buf[role], preferred_element_type=F32))
    copies = deal(send_small, recv_small, sems[0], sems[1], "dp", ndp)
    block = min(cols, 1024)
    for role in (0, 1):
        target, landing = ((send_gate, recv_gate), (send_val, recv_val))[role]
        load_in[role].wait()
        for at in range(0, cols, block):
            put(
                target,
                at,
                jnp.dot(lhs, w_in_buf[role, :, at : at + block], preferred_element_type=F32),
            )
        copies += deal(target, landing, sems[2 + 2 * role], sems[3 + 2 * role], "dp", ndp)
    for copy in copies:
        copy.wait()

    def total(mine, others):
        acc = mine[me].astype(F32)
        for k in range(1, ndp):
            acc = acc + others[k].astype(F32)
        return acc

    small = total(send_small, recv_small)
    own_sq = small[:, 2 * vec_cols + heads : 2 * vec_cols + heads + 1]
    scale = lax.rsqrt(own_sq * (1.0 / MODEL_WIDTH) + EPS)
    for role in range(2):
        vecs_ref[role] = (small[:, role * vec_cols : (role + 1) * vec_cols] * scale).astype(BF16)
    step_ref[...] = small[:, 2 * vec_cols : 2 * vec_cols + heads] * scale
    proj_ref[0] = (total(send_gate, recv_gate) * scale).astype(BF16)
    proj_ref[1] = (total(send_val, recv_val) * scale).astype(BF16)


def first_kernel(
    ntp, ndp, x_ref, gain_ref, w_step_ref, w_in_ref, w_vec_ref,
    proj_ref, vecs_ref, step_ref, all_ref,
    w_in_buf, w_vec_buf, lhs_buf, landed, send_gate, send_val, send_small,
    recv_gate, recv_val, recv_small, load_sem, ssem_x, rsem_x, *sems,
):
    rows_t = x_ref.shape[0]
    load_vec = pltpu.make_async_copy(w_vec_ref.at[0], w_vec_buf, load_sem.at[0])
    load_vec.start()
    load_in = []
    for role in range(2):
        copy = pltpu.make_async_copy(w_in_ref.at[0, role], w_in_buf.at[role], load_sem.at[1 + role])
        copy.start()
        load_in.append(copy)
    greet((("tp", ntp), ("dp", ndp)))
    copies = spread(x_ref, landed, ssem_x, rsem_x, "tp", ntp)
    landed[lax.axis_index("tp")] = x_ref[...]
    gain = gain_ref[...].astype(F32)[0:1]
    for copy in copies:
        copy.wait()
    squares = []
    for i in range(ntp):
        part = landed[i]
        all_ref[i] = part
        part = part.astype(F32)
        squares.append(jnp.sum(part * part, axis=1, keepdims=True))
        lhs_buf[i * rows_t : (i + 1) * rows_t, :] = part * gain
    squares = jnp.concatenate(squares, axis=0)
    project(
        0, ndp, proj_ref.shape[1], lhs_buf[...].astype(BF16), squares, (w_in_buf, w_vec_buf),
        (load_in, load_vec), w_step_ref, (send_gate, send_val, send_small),
        (recv_gate, recv_val, recv_small), sems, (proj_ref, vecs_ref, step_ref),
    )


def gather_normed(ndp, normed_ref, held, lhs_out, send_sem, recv_sem):
    rows_d = normed_ref.shape[0]
    copies = spread(normed_ref, held, send_sem, recv_sem, "dp", ndp)
    held[lax.axis_index("dp")] = normed_ref[...]
    for copy in copies:
        copy.wait()
    for i in range(ndp):
        lhs_out[i * rows_d : (i + 1) * rows_d, :] = held[i].astype(F32)
    return lhs_out[...].astype(BF16)


def middle_kernel(
    layer, ntp, ndp, normed_ref, old_ref, gain_ref, w_step_ref, w_out_ref, w_in_ref, w_vec_ref,
    proj_ref, vecs_ref, step_ref, all_ref,
    w_out_buf, w_in_buf, w_vec_buf, lhs_out, lhs_buf, held, part_out, parts_in,
    send_gate, send_val, send_small, recv_gate, recv_val, recv_small,
    load_sem, ssem_n, rsem_n, ssem_o, rsem_o, *sems,
):
    rows_t = old_ref.shape[1]
    load_out = pltpu.make_async_copy(w_out_ref.at[layer - 1], w_out_buf, load_sem.at[3])
    load_out.start()
    load_vec = pltpu.make_async_copy(w_vec_ref.at[layer], w_vec_buf, load_sem.at[0])
    load_vec.start()
    load_in = []
    for role in range(2):
        copy = pltpu.make_async_copy(
            w_in_ref.at[layer, role], w_in_buf.at[role], load_sem.at[1 + role]
        )
        copy.start()
        load_in.append(copy)
    greet((("tp", ntp), ("dp", ndp)))
    lhs = gather_normed(ndp, normed_ref, held, lhs_out, ssem_n, rsem_n)
    gain = gain_ref[...].astype(F32)[layer : layer + 1]
    load_out.wait()
    part_out[...] = jnp.dot(lhs, w_out_buf[...], preferred_element_type=F32).astype(BF16)
    copies = deal(part_out, parts_in, ssem_o, rsem_o, "tp", ntp, whole=True)
    for copy in copies:
        copy.wait()
    acc = part_out[...].astype(F32)
    for k in range(1, ntp):
        acc = acc + parts_in[k].astype(F32)
    squares = []
    for i in range(ntp):
        part = (old_ref[i].astype(F32) + acc[i * rows_t : (i + 1) * rows_t]).astype(BF16)
        all_ref[i] = part
        part = part.astype(F32)
        squares.append(jnp.sum(part * part, axis=1, keepdims=True))
        lhs_buf[i * rows_t : (i + 1) * rows_t, :] = part * gain
    squares = jnp.concatenate(squares, axis=0)
    project(
        layer, ndp, proj_ref.shape[1], lhs_buf[...].astype(BF16), squares, (w_in_buf, w_vec_buf),
        (load_in, load_vec), w_step_ref, (send_gate, send_val, send_small),
        (recv_gate, recv_val, recv_small), sems, (proj_ref, vecs_ref, step_ref),
    )


def last_kernel(
    layer, ntp, ndp, normed_ref, old_ref, w_out_ref, out_ref,
    w_out_buf, lhs_out, held, send_out, recv_out, load_sem, ssem_n, rsem_n, ssem_o, rsem_o,
):
    rows_t = old_ref.shape[1]
    load_out = pltpu.make_async_copy(w_out_ref.at[layer], w_out_buf, load_sem)
    load_out.start()
    greet((("tp", ntp), ("dp", ndp)))
    lhs = gather_normed(ndp, normed_ref, held, lhs_out, ssem_n, rsem_n)
    load_out.wait()
    acc = jnp.dot(lhs, w_out_buf[...], preferred_element_type=F32)
    for i in range(ntp):
        send_out[i] = acc[i * rows_t : (i + 1) * rows_t].astype(BF16)
    me = lax.axis_index("tp")
    copies = deal(send_out, recv_out, ssem_o, rsem_o, "tp", ntp)
    for copy in copies:
        copy.wait()
    acc = send_out[me].astype(F32)
    for k in range(1, ntp):
        acc = acc + recv_out[k].astype(F32)
    out_ref[...] = (old_ref[me].astype(F32) + acc).astype(BF16)


VMEM = pl.BlockSpec(memory_space=pltpu.VMEM)
HBM = pl.BlockSpec(memory_space=pl.ANY)


def sizes_of(tokens, w_in, w_vec, w_step, ntp, ndp):
    rows_t, width = tokens.shape
    batch = rows_t * ntp
    return rows_t, width, batch, batch // ndp, w_in.shape[3], w_vec.shape[3], w_step.shape[2]


def dma(n):
    return pltpu.SemaphoreType.DMA((n,))


def mixer_scratch(width, cols, vcols, heads, rows_d, ndp):
    small = 2 * vcols + heads + 128
    return [
        pltpu.VMEM((2, width, cols), BF16),
        pltpu.VMEM((2, width, vcols), BF16),
    ], [
        pltpu.VMEM((ndp, rows_d, cols), BF16),
        pltpu.VMEM((ndp, rows_d, cols), BF16),
        pltpu.VMEM((ndp, rows_d, small), BF16),
        pltpu.VMEM((ndp, rows_d, cols), BF16),
        pltpu.VMEM((ndp, rows_d, cols), BF16),
        pltpu.VMEM((ndp, rows_d, small), BF16),
    ]


def first_call(ntp, ndp, tokens, mix_gain, w_step, w_in, w_vec):
    rows_t, width, batch, rows_d, cols, vcols, heads = sizes_of(
        tokens, w_in, w_vec, w_step, ntp, ndp
    )
    bufs, wires = mixer_scratch(width, cols, vcols, heads, rows_d, ndp)
    return pl.pallas_call(
        functools.partial(first_kernel, ntp, ndp),
        out_shape=(
            jax.ShapeDtypeStruct((2, rows_d, cols), BF16),
            jax.ShapeDtypeStruct((2, rows_d, vcols), BF16),
            jax.ShapeDtypeStruct((rows_d, heads), F32),
            jax.ShapeDtypeStruct((ntp, rows_t, width), BF16),
        ),
        in_specs=[VMEM, VMEM, VMEM, HBM, HBM],
        out_specs=(VMEM,) * 4,
        scratch_shapes=bufs
        + [pltpu.VMEM((batch, width), F32), pltpu.VMEM((ntp, rows_t, width), BF16)]
        + wires
        + [dma(3), dma(ntp), dma(ntp)]
        + [dma(ndp)] * 6,
        compiler_params=pltpu.CompilerParams(collective_id=0, has_side_effects=True),
    )(tokens, mix_gain, w_step, w_in, w_vec)


def middle_call(layer, ntp, ndp, tokens, normed, old, mix_gain, w_step, w_out, w_in, w_vec):
    rows_t, width, batch, rows_d, cols, vcols, heads = sizes_of(
        tokens, w_in, w_vec, w_step, ntp, ndp
    )
    bufs, wires = mixer_scratch(width, cols, vcols, heads, rows_d, ndp)
    return pl.pallas_call(
        functools.partial(middle_kernel, layer, ntp, ndp),
        out_shape=(
            jax.ShapeDtypeStruct((2, rows_d, cols), BF16),
            jax.ShapeDtypeStruct((2, rows_d, vcols), BF16),
            jax.ShapeDtypeStruct((rows_d, heads), F32),
            jax.ShapeDtypeStruct((ntp, rows_t, width), BF16),
        ),
        in_specs=[VMEM, VMEM, VMEM, VMEM, HBM, HBM, HBM],
        out_specs=(VMEM,) * 4,
        scratch_shapes=[pltpu.VMEM((cols, width), BF16)]
        + bufs
        + [
            pltpu.VMEM((batch, cols), F32),
            pltpu.VMEM((batch, width), F32),
            pltpu.VMEM((ndp, rows_d, cols), BF16),
            pltpu.VMEM((batch, width), BF16),
            pltpu.VMEM((ntp, batch, width), BF16),
        ]
        + wires
        + [dma(4), dma(ndp), dma(ndp), dma(ntp), dma(ntp)]
        + [dma(ndp)] * 6,
        compiler_params=pltpu.CompilerParams(collective_id=layer, has_side_effects=True),
    )(normed, old, mix_gain, w_step, w_out, w_in, w_vec)


def last_call(layer, ntp, ndp, normed, old, w_out):
    _, rows_t, width = old.shape
    rows_d, cols = normed.shape
    batch = rows_t * ntp
    return pl.pallas_call(
        functools.partial(last_kernel, layer, ntp, ndp),
        out_shape=jax.ShapeDtypeStruct((rows_t, width), BF16),
        in_specs=[VMEM, VMEM, HBM],
        out_specs=VMEM,
        scratch_shapes=[
            pltpu.VMEM((cols, width), BF16),
            pltpu.VMEM((batch, cols), F32),
            pltpu.VMEM((ndp, rows_d, cols), BF16),
            pltpu.VMEM((ntp, rows_t, width), BF16),
            pltpu.VMEM((ntp, rows_t, width), BF16),
            pltpu.SemaphoreType.DMA,
            dma(ndp), dma(ndp), dma(ntp), dma(ntp),
        ],
        compiler_params=pltpu.CompilerParams(collective_id=layer + 1, has_side_effects=True),
    )(normed, old, w_out)


def head_step(
    layer, proj, vecs, step_all, conv_weight, conv_vec, conv_state, vec_state, ssm_state,
    step_bias, decay_log, skip_gain, out_gain,
):
    local_rows, columns = proj.shape[1:]
    vec_columns = vecs.shape[2]
    local_heads = ssm_state.shape[2]
    head_start = lax.axis_index("tp") * local_heads
    step_raw = lax.dynamic_slice_in_dim(step_all, head_start, local_heads, 1)
    window = jnp.concatenate([conv_state[layer], proj[1][:, None, :]], axis=1)
    new_conv = window[:, 1:, :]
    values_sum = jnp.sum(
        window.astype(jnp.float32) * conv_weight[layer].astype(jnp.float32)[None, :, :], axis=1
    )
    fresh = vecs[:, :, None, :]
    vec_window = jnp.concatenate([vec_state[layer], fresh], axis=2)
    new_vec = vec_window[:, :, 1:, :]
    vec_sum = jnp.sum(
        vec_window.astype(jnp.float32) * conv_vec[layer].astype(jnp.float32)[:, None, :, :], axis=2
    )
    values = jax.nn.silu(values_sum).reshape(local_rows, local_heads, HEAD_DIM)
    vec_act = jax.nn.silu(vec_sum)
    local_groups = vec_columns // STATE_DIM
    repeat = HEAD_COUNT // GROUP_COUNT
    in_vec = jnp.repeat(vec_act[0].reshape(local_rows, local_groups, STATE_DIM), repeat, axis=1)
    out_vec = jnp.repeat(vec_act[1].reshape(local_rows, local_groups, STATE_DIM), repeat, axis=1)
    step = jax.nn.softplus(step_raw + step_bias[layer][None, :])
    decay = jnp.exp(-step * jnp.exp(decay_log[layer])[None, :])
    state = (
        decay[:, :, None, None] * ssm_state[layer]
        + (step[:, :, None] * values)[..., None] * in_vec[:, :, None, :]
    )
    read = jnp.einsum("bhpn,bhn->bhp", state, out_vec) + skip_gain[layer][None, :, None] * values
    mixed = read.reshape(local_rows, columns) * jax.nn.silu(proj[0].astype(jnp.float32))
    grouped = mixed.reshape(local_rows, local_groups, columns // local_groups)
    grouped = grouped * lax.rsqrt(jnp.mean(grouped * grouped, axis=2, keepdims=True) + EPS)
    normed = (grouped.reshape(local_rows, columns) * out_gain[layer].astype(jnp.float32)).astype(
        jnp.bfloat16
    )
    return (normed, new_conv, new_vec, (decay, step[:, :, None] * values, in_vec))


def shards(
    ntp,
    ndp,
    tokens,
    w_in,
    w_vec,
    w_step,
    conv_weight,
    conv_vec,
    conv_state,
    vec_state,
    ssm_state,
    step_bias,
    decay_log,
    skip_gain,
    mix_gain,
    out_gain,
    w_out,
):
    convs = []
    vec_rows = []
    states = []
    for layer in range(LAYER_COUNT):
        if layer == 0:
            proj, vecs, step_all, rows = first_call(
                ntp, ndp, tokens, mix_gain, w_step, w_in, w_vec
            )
        else:
            proj, vecs, step_all, rows = middle_call(
                layer, ntp, ndp, tokens, normed, rows, mix_gain, w_step, w_out, w_in, w_vec
            )
        normed, conv_next, vec_next, state_next = head_step(
            layer, proj, vecs, step_all, conv_weight, conv_vec, conv_state, vec_state,
            ssm_state, step_bias, decay_log, skip_gain, out_gain,
        )
        convs.append(conv_next)
        vec_rows.append(vec_next)
        states.append(state_next)
    current = last_call(LAYER_COUNT - 1, ntp, ndp, normed, rows, w_out)
    decays, drives, inputs = (jnp.stack(parts) for parts in zip(*states))
    new_ssm = (
        decays[..., None, None] * ssm_state + drives[..., None] * inputs[:, :, :, None, :]
    )
    return (current, jnp.stack(convs), jnp.stack(vec_rows), new_ssm)


def solution(mesh):
    placed = (
        P(("grp", "tp"), "dp"),
        P(None, None, "dp", "tp"),
        P(None, None, "dp", "tp"),
        P(None, "dp", None),
        P(None, None, "tp"),
        P(None, None, None, "tp"),
        P(None, ("grp", "dp"), None, "tp"),
        P(None, None, ("grp", "dp"), None, "tp"),
        P(None, ("grp", "dp"), "tp", None, None),
        P(None, "tp"),
        P(None, "tp"),
        P(None, "tp"),
        P(None, "dp"),
        P(None, "tp"),
        P(None, "tp", "dp"),
    )
    return jax.shard_map(
        functools.partial(shards, mesh.shape["tp"], mesh.shape["dp"]),
        mesh=mesh,
        in_specs=placed,
        out_specs=(
            P(("grp", "tp"), "dp"),
            P(None, ("grp", "dp"), None, "tp"),
            P(None, None, ("grp", "dp"), None, "tp"),
            P(None, ("grp", "dp"), "tp", None, None),
        ),
        check_vma=False,
    )
```

profile of v0, /device:TPU:0, one launch (start us, length us, event | category | flops | bytes accessed | tf_op | source)
XLA Modules:
  0.0 95.6 jit_solution(13292287167607434752)
XLA Ops:
  0.6 0.8 slice_bitcast_fusion.9
  1.4 0.8 exponential_bitcast_fusion
  2.2 0.8 slice_bitcast_fusion.8
  2.9 0.8 slice_convert_fusion.2
  3.7 0.7 bitcast_convert_fusion.2
  4.4 0.7 bitcast_convert_fusion
  5.2 0.8 slice_bitcast_fusion.2
  6.0 0.0 copy-start
  6.0 19.5 %shard_map.174 = (bf16[2,8,2048]{2,1,0:T(8,128)(2,1)}, bf16[2,8,512]{2,1,0:T(8,128)(2,1)}, f32[8,128]{1,0:T(8,128)}, bf16[4,8,1024]{2,1,0:T(8,128)(2,1)}) custom-call(bf16[8,1024]{1,0:T(8,128)(2,1)} %x_ref.1, bf16[2,1024]{1,0:T(2,128)(2,1)} %gain_ref.3, bf16[2,1024,128]{2,1,0:T(8,128)(2,1)} %w_step_ref.3, bf16[2,2,1024,2048]{3,2,1,0:T(8,128)(2,1)} %w_in_ref.3, ...), custom_call_target="tpu_custom_call" | custom-call | tf_op jit(solution)/shard_map/pallas_call | solution.py:278
  25.5 0.0 copy-start.2
  25.5 0.8 multiply_exponential_fusion.1
  26.3 0.7 multiply_reduce_fusion.5
  27.1 0.8 slice_bitcast_fusion.5
  27.9 0.1 reshape.186
  28.0 0.0 copy-done
  28.0 0.1 reduce_sum.77
  28.1 0.1 reduce_sum.88
  28.2 0.1 broadcast_multiply_fusion.1
  28.4 5.7 %fusion.4 = f32[8,32,1,64]{3,2,1,0:T(1,128)S(1)} fusion(f32[8,32,128,1]{2,3,1,0:T(1,128)S(1)} %bitcast.137, f32[2,8,32,64,128]{4,3,2,1,0:T(8,128)} %param.23, f32[8,32,128]{2,1,0:T(8,128)S(1)} %get-tuple-element.43, f32[8,32,64]{2,1,0:T(8,128)S(1)} %broadcast_multiply_fusion.1, f32[8,32]{1,0:T(8,128)S(1)} %get-tuple-element.26), kind=kOutput, calls=%fused_computation.6 | convolution fusion | flops 10485760 | bytes 8782848 | tf_op jit(solution)/shard_map/bhpn,bhn->bhp/dot_general | solution.py:382
  34.1 0.2 multiply_reduce_fusion.4
  34.3 0.1 reduce_sum.80
  34.4 0.1 reduce_sum.81
  34.4 0.1 copy.37
  34.5 0.1 mul.365
  34.6 0.1 reshape.180
  34.7 0.0 copy-done.2
  34.7 0.7 fusion.32.normed_ref
  35.4 0.0 copy-start.4
  35.4 23.2 %shard_map.175 = (bf16[2,8,2048]{2,1,0:T(8,128)(2,1)}, bf16[2,8,512]{2,1,0:T(8,128)(2,1)}, f32[8,128]{1,0:T(8,128)}, bf16[4,8,1024]{2,1,0:T(8,128)(2,1)}) custom-call(bf16[8,2048]{1,0:T(8,128)(2,1)} %fusion.32.normed_ref, bf16[4,8,1024]{2,1,0:T(8,128)(2,1)} %get-tuple-element.15.old_ref, bf16[2,1024]{1,0:T(2,128)(2,1)} %gain_ref.3, ...), custom_call_target="tpu_custom_call" | custom-call | tf_op jit(solution)/shard_map/pallas_call | solution.py:302
  58.6 0.0 copy-start.1
  58.6 0.8 multiply_exponential_fusion
  59.4 0.7 multiply_reduce_fusion.3
  60.2 0.0 copy-done.4
  60.2 0.7 fusion.35
  60.9 0.7 pad_maximum_fusion.5
  61.6 0.8 slice_bitcast_fusion.4
  62.5 0.7 pad_maximum_fusion.2
  63.2 0.1 reshape.191
  63.3 0.1 reduce_sum.83
  63.3 0.1 reduce_sum.89
  63.4 0.1 multiply_multiply_fusion
  63.6 0.1 broadcast_multiply_fusion
  63.7 5.7 %fusion.1 = f32[8,32,1,64]{3,2,1,0:T(1,128)S(1)} fusion(f32[8,32,128,1]{2,3,1,0:T(1,128)S(1)} %bitcast.136, f32[2,8,32,64,128]{4,3,2,1,0:T(8,128)} %param.23, f32[8,32,128]{2,1,0:T(8,128)S(1)} %get-tuple-element.45, f32[8,32,64]{2,1,0:T(8,128)S(1)} %broadcast_multiply_fusion, f32[8,32]{1,0:T(8,128)S(1)} %get-tuple-element.22), kind=kOutput, calls=%fused_computation.3 | convolution fusion | flops 10485760 | bytes 8782848 | tf_op jit(solution)/shard_map/bhpn,bhn->bhp/dot_general | solution.py:382
  69.5 0.2 multiply_reduce_fusion.2
  69.7 0.1 reduce_sum.86
  69.8 0.1 reduce_sum.87
  69.8 0.1 copy.38
  69.9 0.1 mul.399
  70.0 0.1 reshape.182
  70.1 0.0 copy-done.1
  70.1 0.7 fusion.33.normed_ref
  70.8 11.2 %shard_map.176 = bf16[8,1024]{1,0:T(8,128)(2,1)} custom-call(bf16[8,2048]{1,0:T(8,128)(2,1)} %fusion.33.normed_ref, bf16[4,8,1024]{2,1,0:T(8,128)(2,1)} %get-tuple-element.19.old_ref, bf16[2,2048,1024]{2,1,0:T(8,128)(2,1)} %w_out_ref.3), custom_call_target="tpu_custom_call" | custom-call | tf_op jit(solution)/shard_map/pallas_call | solution.py:332
  82.0 0.0 copy-start.3
  82.0 13.0 %multiply_add_fusion = f32[2,8,32,64,128]{4,3,2,1,0:T(8,128)} fusion(f32[2,8,32,64,128]{4,3,2,1,0:T(8,128)} %param.23, f32[2,8,32,128]{3,2,1,0:T(8,128)S(1)} %pad_maximum_fusion.1, f32[2,8,32,64]{3,2,1,0:T(8,128)S(1)} %pad_maximum_fusion, f32[2,8,32]{2,1,0:T(8,128)S(1)} %pad_maximum_fusion.8), kind=kLoop, calls=%fused_computation | loop fusion | flops 12582912 | bytes 33949696 | tf_op jit(solution)/shard_map/add | solution.py:433
  95.0 0.0 copy-done.3
  95.0 0.6 copy.40
  (21 shorter events, 0.3 us)
Async XLA Ops:
  6.0 22.0 %copy-start = (bf16[2,8,3,2048]{3,1,2,0:T(8,128)(2,1)S(1)}, bf16[2,8,3,2048]{3,1,2,0:T(8,128)(2,1)}, u32[]{:S(2)}) copy-start(bf16[2,8,3,2048]{3,1,2,0:T(8,128)(2,1)} %param.21) | copy-start | bytes 589828
  25.5 9.3 %copy-start.2 = (bf16[2,8,2048]{2,1,0:T(8,128)(2,1)S(1)}, bf16[2,8,2048]{2,1,0:T(8,128)(2,1)}, u32[]{:S(2)}) copy-start(bf16[2,8,2048]{2,1,0:T(8,128)(2,1)} %get-tuple-element.13) | copy-start | bytes 196612
  35.4 24.8 %copy-start.4 = (bf16[2,8,512]{2,1,0:T(8,128)(2,1)S(1)}, bf16[2,8,512]{2,1,0:T(8,128)(2,1)}, u32[]{:S(2)}) copy-start(bf16[2,8,512]{2,1,0:T(8,128)(2,1)} %get-tuple-element.14) | copy-start | bytes 49156
  58.6 11.5 %copy-start.1 = (bf16[2,8,2048]{2,1,0:T(8,128)(2,1)S(1)}, bf16[2,8,2048]{2,1,0:T(8,128)(2,1)}, u32[]{:S(2)}) copy-start(bf16[2,8,2048]{2,1,0:T(8,128)(2,1)} %get-tuple-element.17) | copy-start | bytes 196612
  82.0 13.0 %copy-start.3 = (bf16[8,1024]{1,0:T(8,128)(2,1)S(1)}, bf16[8,1024]{1,0:T(8,128)(2,1)}, u32[]{:S(2)}) copy-start(bf16[8,1024]{1,0:T(8,128)(2,1)} %shard_map.176) | copy-start | bytes 49156
where the time goes:
time: 96.6 us; the launch traced here: 95.6 us
  Pallas kernels  53.8 us (56%)
  other arithmetic  24.4 us (25%)
  matrix products  11.4 us (12%)
  local copies, waits for them, and re-layouts  5.04 us (5%)
    pallas_call x1, Pallas kernels, middle_call(): pl.pallas_call(functools.partial(middle_kernel, layer, ntp, ndp), out_sha...  23.2 us
    pallas_call x1, Pallas kernels, first_call(): pl.pallas_call(functools.partial(first_kernel, ntp, ndp), out_shape=(jax....  19.5 us
    add x1, other arithmetic, shards(): decays[..., None, None] * ssm_state  13 us
    dot_general x2, matrix products, head_step(): jnp.einsum('bhpn,bhn->bhp', state, out_vec)  11.4 us
    pallas_call x1, Pallas kernels, last_call(): pl.pallas_call(functools.partial(last_kernel, layer, ntp, ndp), out_shape...  11.2 us
    another operation x4, other arithmetic, shards(): return (current, jnp.stack(convs), jnp.stack(vec_rows), new_ssm)  2.1 us

commit v1 on v0

v1 whole, which is shorter than its diff:
```python
import functools

import jax
import jax.numpy as jnp
from jax import lax
from jax.experimental import pallas as pl
from jax.experimental.pallas import tpu as pltpu
from jax.sharding import PartitionSpec as P

MODEL_WIDTH = 4096
HEAD_DIM = 64
STATE_DIM = 128
LANES = 128
LAYER_COUNT = 2

EPS = 1e-06
F32 = jnp.float32
BF16 = jnp.bfloat16


def remote(src, dst, send_sem, recv_sem, axis, target):
    return pltpu.make_async_remote_copy(
        src_ref=src,
        dst_ref=dst,
        send_sem=send_sem,
        recv_sem=recv_sem,
        device_id={axis: target},
        device_id_type=pl.DeviceIdType.MESH,
    )


def greet(sizes):
    barrier = pltpu.get_barrier_semaphore()
    count = 0
    for axis, n in sizes:
        me = lax.axis_index(axis)
        for k in range(1, n):
            pl.semaphore_signal(
                barrier,
                inc=1,
                device_id={axis: lax.rem(me + k, n)},
                device_id_type=pl.DeviceIdType.MESH,
            )
            count += 1
    pl.semaphore_wait(barrier, count)


def silu(v):
    return v / (1.0 + jnp.exp(-v))


def softplus(v):
    return jnp.maximum(v, 0.0) + jnp.log1p(jnp.exp(-jnp.abs(v)))


def expand(per_head, at, rows):
    per = LANES // HEAD_DIM
    lane = lax.broadcasted_iota(jnp.int32, (rows, LANES), 1)
    out = jnp.broadcast_to(per_head[:, at : at + 1], (rows, LANES))
    for j in range(1, per):
        other = jnp.broadcast_to(per_head[:, at + j : at + j + 1], (rows, LANES))
        out = jnp.where(lane >= j * HEAD_DIM, other, out)
    return out


def mixer_kernel(
    ntp, ndp,
    x_ref, gain_hbm, w_step_hbm, w_in_hbm, w_vec_hbm, w_out_hbm, conv_w_hbm, conv_v_hbm,
    conv_hbm, vec_hbm, ssm_hbm, bias_hbm, decay_hbm, skip_hbm, out_gain_hbm,
    tok_ref, new_conv, new_vec, ssm_ref,
    w_step, w_in, w_vec, w_out, gain, conv_w, conv_v, conv_s, vec_s, bias, decay_log, skip, out_gain,
    landed, lhs_buf, send_small, recv_small, send_proj, recv_proj,
    ins_buf, outs_buf, read_buf, drive_pad, drive_t, decay_pad, decay_t,
    held, lhs_out, part_out, parts_in, rows_buf, send_out, recv_out,
    small_sem, weight_sem, ssm_sem, ssem_x, rsem_x, ssem_s, rsem_s, ssem_p, rsem_p,
    ssem_n, rsem_n, ssem_o, rsem_o, ssem_f, rsem_f,
):
    rows_t, width = x_ref.shape
    batch = rows_t * ntp
    rows_d = batch // ndp
    cols = w_in.shape[3]
    vcols = w_vec.shape[3]
    heads = w_step.shape[2]
    local_heads = ssm_ref.shape[2]
    groups = vcols // STATE_DIM
    span = cols // groups
    group_heads = local_heads // groups
    block = min(cols, 1024)
    blocks = cols // block
    tp = lax.axis_index("tp")
    dp = lax.axis_index("dp")
    pending = []

    def load(src, dst, sem):
        copy = pltpu.make_async_copy(src, dst, sem)
        copy.start()
        return copy

    def load_weights(layer):
        vec = load(w_vec_hbm.at[layer], w_vec.at[layer], weight_sem.at[layer, 0])
        step = load(w_step_hbm.at[layer], w_step.at[layer], weight_sem.at[layer, 1])
        return vec, step, [
            load(w_in_hbm.at[layer, role], w_in.at[layer, role], weight_sem.at[layer, 2 + role])
            for role in (1, 0)
        ]

    smalls = [
        load(src, dst, small_sem.at[i])
        for i, (src, dst) in enumerate(
            (
                (gain_hbm, gain), (conv_w_hbm, conv_w), (conv_v_hbm, conv_v),
                (conv_hbm, conv_s), (vec_hbm, vec_s), (bias_hbm, bias),
                (decay_hbm, decay_log), (skip_hbm, skip), (out_gain_hbm, out_gain),
            )
        )
    ]
    weights = [load_weights(0)]
    greet((("tp", ntp), ("dp", ndp)))
    gathers = []
    for k in range(1, ntp):
        copy = remote(
            x_ref, landed.at[tp], ssem_x.at[k], rsem_x.at[k], "tp", lax.rem(tp + k, ntp)
        )
        copy.start()
        gathers.append(copy)
    landed[tp] = x_ref[...]
    drive_pad[...] = jnp.zeros_like(drive_pad)
    decay_pad[...] = jnp.zeros_like(decay_pad)
    for copy in smalls:
        copy.wait()
    for copy in gathers:
        copy.wait()
    out_loads = []
    state_loads = []

    def project(layer, rows):
        scale_row = gain[...].astype(F32)[layer : layer + 1]
        squares = []
        for i in range(ntp):
            part = rows(i)
            squares.append(jnp.sum(part * part, axis=1, keepdims=True))
            lhs_buf[i * rows_t : (i + 1) * rows_t, :] = part * scale_row
        squares = jnp.concatenate(squares, axis=0)
        lhs = lhs_buf[...].astype(BF16)
        load_vec, load_step, load_in = weights[layer]

        def put(target, at, acc):
            for p in range(ndp):
                target[p, :, at : at + acc.shape[1]] = acc[p * rows_d : (p + 1) * rows_d].astype(
                    BF16
                )

        def deal(target, landing, ssem, rsem):
            copies = []
            for k in range(ndp - 1, 0, -1):
                peer = lax.rem(dp + k, ndp)
                copy = remote(target.at[peer], landing.at[k], ssem.at[k], rsem.at[k], "dp", peer)
                copy.start()
                copies.append(copy)
            pending.extend(copies)
            return copies

        load_step.wait()
        load_vec.wait()
        small = jnp.dot(lhs, w_step[layer], preferred_element_type=F32)
        small = pltpu.roll(small, lax.rem(heads - tp * local_heads, heads), 1)
        lane = lax.broadcasted_iota(jnp.int32, small.shape, 1)
        small = jnp.where(lane == local_heads, jnp.broadcast_to(squares, small.shape), small)
        put(send_small.at[layer], 2 * vcols, small)
        for role in range(2):
            put(
                send_small.at[layer], role * vcols,
                jnp.dot(lhs, w_vec[layer, role], preferred_element_type=F32),
            )
        flights = [
            deal(send_small.at[layer], recv_small.at[layer], ssem_s.at[layer], rsem_s.at[layer])
        ]
        for j, role in enumerate((1, 0)):
            load_in[j].wait()
            for b in range(blocks):
                c = j * blocks + b
                acc = jnp.dot(
                    lhs, w_in[layer, role, :, b * block : (b + 1) * block],
                    preferred_element_type=F32,
                )
                put(send_proj.at[layer, c], 0, acc)
                flights.append(
                    deal(
                        send_proj.at[layer, c], recv_proj.at[layer, c],
                        ssem_p.at[layer, c], rsem_p.at[layer, c],
                    )
                )
        return flights

    def total(mine, others):
        acc = mine[dp].astype(F32)
        for k in range(1, ndp):
            acc = acc + others[k].astype(F32)
        return acc

    def head_step(layer, flights):
        for copy in flights[0]:
            copy.wait_recv()
        small = total(send_small.at[layer], recv_small.at[layer])
        own_sq = small[:, 2 * vcols + local_heads : 2 * vcols + local_heads + 1]
        scale = lax.rsqrt(own_sq * (1.0 / MODEL_WIDTH) + EPS)
        taps_v = conv_v[layer].astype(F32)
        acts = []
        for role in range(2):
            fresh = (small[:, role * vcols : (role + 1) * vcols] * scale).astype(BF16)
            acc = fresh.astype(F32) * taps_v[role, 3:4]
            for i in range(3):
                acc = acc + vec_s[layer, role, i].astype(F32) * taps_v[role, i : i + 1]
            new_vec[layer, role, 0] = vec_s[layer, role, 1]
            new_vec[layer, role, 1] = vec_s[layer, role, 2]
            new_vec[layer, role, 2] = fresh
            acts.append(silu(acc))
        in_vec, out_vec = acts
        step = softplus(
            small[:, 2 * vcols : 2 * vcols + local_heads] * scale + bias[layer : layer + 1]
        )
        decay = jnp.exp(-step * jnp.exp(decay_log[layer : layer + 1]))
        decay_pad[0:rows_d, 0:local_heads] = decay
        decay_t[...] = jnp.transpose(decay_pad[...])
        state_loads[layer].wait()
        row = lax.broadcasted_iota(jnp.int32, (rows_d, STATE_DIM), 0)
        skips = jnp.broadcast_to(skip[layer : layer + 1], (rows_d, local_heads))
        for g in range(groups):
            ins_buf[g] = in_vec[:, g * STATE_DIM : (g + 1) * STATE_DIM]
            outs_buf[g] = out_vec[:, g * STATE_DIM : (g + 1) * STATE_DIM]
            out_g = outs_buf[g]
            acc = jnp.zeros((rows_d, span), F32)
            for r in range(rows_d):
                mine = jnp.where(row == r, out_g, 0.0)
                state = ssm_ref[layer, r, g * group_heads : (g + 1) * group_heads]
                acc = acc + lax.dot_general(
                    mine, state.reshape(span, STATE_DIM), (((1,), (1,)), ((), ())),
                    preferred_element_type=F32,
                )
            read_buf[:, g * span : (g + 1) * span] = acc
        taps = conv_w[layer].astype(F32)
        for b in range(blocks):
            for copy in flights[1 + b]:
                copy.wait_recv()
            cut = slice(b * block, (b + 1) * block)
            fresh = (total(send_proj.at[layer, b], recv_proj.at[layer, b]) * scale).astype(BF16)
            acc = fresh.astype(F32) * taps[3:4, cut]
            for i in range(3):
                acc = acc + conv_s[layer, i, :, cut].astype(F32) * taps[i : i + 1, cut]
            new_conv[layer, 0, :, cut] = conv_s[layer, 1, :, cut]
            new_conv[layer, 1, :, cut] = conv_s[layer, 2, :, cut]
            new_conv[layer, 2, :, cut] = fresh
            values = silu(acc)
            for at in range(0, block, LANES):
                lane0 = b * block + at
                head = lane0 // HEAD_DIM
                g = lane0 // span
                inner = jnp.sum(
                    in_vec[:, g * STATE_DIM : (g + 1) * STATE_DIM]
                    * out_vec[:, g * STATE_DIM : (g + 1) * STATE_DIM],
                    axis=1, keepdims=True,
                )
                v = values[:, at : at + LANES]
                drive = expand(step, head, rows_d) * v
                drive_pad[0:rows_d, lane0 : lane0 + LANES] = drive
                read_buf[:, lane0 : lane0 + LANES] = (
                    expand(decay, head, rows_d) * read_buf[:, lane0 : lane0 + LANES]
                    + drive * inner
                    + expand(skips, head, rows_d) * v
                )
        gain_row = out_gain[...].astype(F32)[layer : layer + 1]
        flown = []
        for b in range(blocks):
            c = blocks + b
            for copy in flights[1 + c]:
                copy.wait_recv()
            fresh = (total(send_proj.at[layer, c], recv_proj.at[layer, c]) * scale).astype(BF16)
            mixed = read_buf[:, b * block : (b + 1) * block] * silu(fresh.astype(F32))
            for at in range(0, block, span):
                cut = slice(b * block + at, b * block + at + span)
                part = mixed[:, at : at + span]
                mean = jnp.mean(part * part, axis=1, keepdims=True)
                held[layer, dp, :, cut] = (
                    part * lax.rsqrt(mean + EPS) * gain_row[:, cut]
                ).astype(BF16)
            copies = []
            for k in range(ndp - 1, 0, -1):
                cut = pl.ds(b * block, block)
                copy = remote(
                    held.at[layer, dp, :, cut], held.at[layer, dp, :, cut],
                    ssem_n.at[layer, b, k], rsem_n.at[layer, b, k], "dp", lax.rem(dp + k, ndp),
                )
                copy.start()
                copies.append(copy)
            pending.extend(copies)
            flown.append(copies)
        return flown

    def update_state(layer):
        for at in range(0, cols, LANES):
            drive_t[at : at + LANES, :] = jnp.transpose(drive_pad[:, at : at + LANES])

        def one_head(h, carry):
            decay_row = decay_t[pl.ds(h, 1), :]
            drive = drive_t[pl.ds(pl.multiple_of(h * HEAD_DIM, HEAD_DIM), HEAD_DIM), :]
            inp = ins_buf[h // group_heads]
            for r in range(rows_d):
                ssm_ref[layer, r, h] = ssm_ref[layer, r, h] * jnp.broadcast_to(
                    decay_row[:, r : r + 1], (HEAD_DIM, STATE_DIM)
                ) + jnp.broadcast_to(drive[:, r : r + 1], (HEAD_DIM, STATE_DIM)) * inp[r : r + 1, :]
            return carry

        lax.fori_loop(0, local_heads, one_head, 0)

    def gather_out(layer, flown):
        out_loads[layer].wait()
        acc = jnp.zeros((batch, width), F32)
        for b in range(blocks):
            for copy in flown[b]:
                copy.wait_recv()
            cut = slice(b * block, (b + 1) * block)
            for i in range(ndp):
                lhs_out[i * rows_d : (i + 1) * rows_d, cut] = held[layer, i, :, cut].astype(F32)
            acc = acc + jnp.dot(
                lhs_out[:, cut].astype(BF16), w_out[layer, cut, :], preferred_element_type=F32
            )
        return acc

    flights = project(0, lambda i: landed[i].astype(F32))
    for layer in range(LAYER_COUNT):
        state_loads.append(load(ssm_hbm.at[layer], ssm_ref.at[layer], ssm_sem.at[layer]))
        out_loads.append(load(w_out_hbm.at[layer], w_out.at[layer], weight_sem.at[layer, 4]))
        flown = head_step(layer, flights)
        last = layer == LAYER_COUNT - 1
        if not last:
            weights.append(load_weights(layer + 1))
        update_state(layer)
        acc = gather_out(layer, flown)
        if last:
            for i in range(ntp):
                send_out[i] = acc[i * rows_t : (i + 1) * rows_t].astype(BF16)
            finals = []
            for k in range(1, ntp):
                peer = lax.rem(tp + k, ntp)
                copy = remote(send_out.at[peer], recv_out.at[k], ssem_f.at[k], rsem_f.at[k], "tp", peer)
                copy.start()
                finals.append(copy)
            for copy in finals:
                copy.wait()
            total_out = send_out[tp].astype(F32)
            for k in range(1, ntp):
                total_out = total_out + recv_out[k].astype(F32)
            tok_ref[...] = (rows_buf[tp].astype(F32) + total_out).astype(BF16)
        else:
            part_out[layer] = acc.astype(BF16)
            parts = []
            for k in range(1, ntp):
                copy = remote(
                    part_out.at[layer], parts_in.at[layer, k], ssem_o.at[layer, k],
                    rsem_o.at[layer, k], "tp", lax.rem(tp + k, ntp),
                )
                copy.start()
                parts.append(copy)
            pending.extend(parts)
            for copy in parts:
                copy.wait_recv()
            acc = part_out[layer].astype(F32)
            for k in range(1, ntp):
                acc = acc + parts_in[layer, k].astype(F32)
            before = landed if layer == 0 else rows_buf

            def rows(i, before=before, acc=acc):
                part = (before[i].astype(F32) + acc[i * rows_t : (i + 1) * rows_t]).astype(BF16)
                rows_buf[i] = part
                return part.astype(F32)

            flights = project(layer + 1, rows)
    for copy in pending:
        copy.wait_send()


def write_kernel(tok, conv, vec, ssm, tok_out, conv_out, vec_out, ssm_out, sem, ssm_sem):
    copies = []
    layers, rows = ssm.shape[:2]
    for l in range(layers):
        for r in range(rows):
            copies.append(
                pltpu.make_async_copy(ssm.at[l, r], ssm_out.at[l, r], ssm_sem.at[l, r])
            )
    for i, (src, dst) in enumerate(((tok, tok_out), (conv, conv_out), (vec, vec_out))):
        copies.append(pltpu.make_async_copy(src, dst, sem.at[i]))
    for copy in copies:
        copy.start()
    for copy in copies:
        copy.wait()


VMEM = pl.BlockSpec(memory_space=pltpu.VMEM)
HBM = pl.BlockSpec(memory_space=pl.ANY)


def dma(*shape):
    return pltpu.SemaphoreType.DMA(shape)


def shards(
    ntp, ndp, tokens, w_in, w_vec, w_step, conv_weight, conv_vec, conv_state, vec_state,
    ssm_state, step_bias, decay_log, skip_gain, mix_gain, out_gain, w_out,
):
    rows_t, width = tokens.shape
    layers = w_in.shape[0]
    batch = rows_t * ntp
    rows_d = batch // ndp
    cols, vcols, heads = w_in.shape[3], w_vec.shape[3], w_step.shape[2]
    groups = vcols // STATE_DIM
    block = min(cols, 1024)
    chunks = 2 * cols // block
    small = 2 * vcols + LANES
    conv_rows = jnp.transpose(conv_state, (0, 2, 1, 3))
    vec_rows = jnp.transpose(vec_state, (0, 1, 3, 2, 4))
    scratch = [
        pltpu.VMEM(w_step.shape, BF16),
        pltpu.VMEM(w_in.shape, BF16),
        pltpu.VMEM(w_vec.shape, BF16),
        pltpu.VMEM(w_out.shape, BF16),
        pltpu.VMEM(mix_gain.shape, BF16),
        pltpu.VMEM(conv_weight.shape, BF16),
        pltpu.VMEM(conv_vec.shape, BF16),
        pltpu.VMEM(conv_rows.shape, BF16),
        pltpu.VMEM(vec_rows.shape, BF16),
        pltpu.VMEM(step_bias.shape, F32),
        pltpu.VMEM(decay_log.shape, F32),
        pltpu.VMEM(skip_gain.shape, F32),
        pltpu.VMEM(out_gain.shape, BF16),
        pltpu.VMEM((ntp, rows_t, width), BF16),
        pltpu.VMEM((batch, width), F32),
        pltpu.VMEM((layers, ndp, rows_d, small), BF16),
        pltpu.VMEM((layers, ndp, rows_d, small), BF16),
        pltpu.VMEM((layers, chunks, ndp, rows_d, block), BF16),
        pltpu.VMEM((layers, chunks, ndp, rows_d, block), BF16),
        pltpu.VMEM((groups, rows_d, STATE_DIM), F32),
        pltpu.VMEM((groups, rows_d, STATE_DIM), F32),
        pltpu.VMEM((rows_d, cols), F32),
        pltpu.VMEM((LANES, cols), F32),
        pltpu.VMEM((cols, LANES), F32),
        pltpu.VMEM((LANES, LANES), F32),
        pltpu.VMEM((LANES, LANES), F32),
        pltpu.VMEM((layers, ndp, rows_d, cols), BF16),
        pltpu.VMEM((batch, cols), F32),
        pltpu.VMEM((layers, batch, width), BF16),
        pltpu.VMEM((layers, ntp, batch, width), BF16),
        pltpu.VMEM((ntp, rows_t, width), BF16),
        pltpu.VMEM((ntp, rows_t, width), BF16),
        pltpu.VMEM((ntp, rows_t, width), BF16),
        dma(9), dma(layers, 5), dma(layers), dma(ntp), dma(ntp),
        dma(layers, ndp), dma(layers, ndp), dma(layers, chunks, ndp), dma(layers, chunks, ndp),
        dma(layers, chunks, ndp), dma(layers, chunks, ndp),
        dma(layers, ntp), dma(layers, ntp), dma(ntp), dma(ntp),
    ]
    results = pl.pallas_call(
        functools.partial(mixer_kernel, ntp, ndp),
        out_shape=(
            pltpu.VMEM(tokens.shape, BF16),
            pltpu.VMEM(conv_rows.shape, BF16),
            pltpu.VMEM(vec_rows.shape, BF16),
            pltpu.VMEM(ssm_state.shape, F32),
        ),
        in_specs=[VMEM] + [HBM] * 14,
        out_specs=(VMEM,) * 4,
        scratch_shapes=scratch,
        compiler_params=pltpu.CompilerParams(
            collective_id=0, has_side_effects=True, vmem_limit_bytes=44 << 20
        ),
    )(
        tokens, mix_gain, w_step, w_in, w_vec, w_out, conv_weight, conv_vec, conv_rows, vec_rows,
        ssm_state, step_bias, decay_log, skip_gain, out_gain,
    )
    new_tokens, new_conv, new_vec, new_ssm = pl.pallas_call(
        write_kernel,
        out_shape=tuple(jax.ShapeDtypeStruct(r.shape, r.dtype) for r in results),
        in_specs=[VMEM] * 4,
        out_specs=(HBM,) * 4,
        scratch_shapes=[dma(3), dma(layers, rows_d)],
        compiler_params=pltpu.CompilerParams(vmem_limit_bytes=8 << 20),
    )(*results)
    return (
        new_tokens,
        jnp.transpose(new_conv, (0, 2, 1, 3)),
        jnp.transpose(new_vec, (0, 1, 3, 2, 4)),
        new_ssm,
    )


def solution(mesh):
    placed = (
        P(("grp", "tp"), "dp"),
        P(None, None, "dp", "tp"),
        P(None, None, "dp", "tp"),
        P(None, "dp", None),
        P(None, None, "tp"),
        P(None, None, None, "tp"),
        P(None, ("grp", "dp"), None, "tp"),
        P(None, None, ("grp", "dp"), None, "tp"),
        P(None, ("grp", "dp"), "tp", None, None),
        P(None, "tp"),
        P(None, "tp"),
        P(None, "tp"),
        P(None, "dp"),
        P(None, "tp"),
        P(None, "tp", "dp"),
    )
    return jax.shard_map(
        functools.partial(shards, mesh.shape["tp"], mesh.shape["dp"]),
        mesh=mesh,
        in_specs=placed,
        out_specs=(
            P(("grp", "tp"), "dp"),
            P(None, ("grp", "dp"), None, "tp"),
            P(None, None, ("grp", "dp"), None, "tp"),
            P(None, ("grp", "dp"), "tp", None, None),
        ),
        check_vma=False,
    )
```

time: 96.6 us -> 58.8 us (0.61)
  other arithmetic: 24.4 us -> 0 us
  matrix products: 11.4 us -> 0 us
  local copies, waits for them, and re-layouts: 5.04 us -> 0 us
  Pallas kernels: 53.8 us -> 57.9 us
    add x1 -> x0, other arithmetic: 13 us -> none  [shards(): decays[..., None, None] * ssm_state]
    dot_general x2 -> x0, matrix products: 11.4 us -> none  [head_step(): jnp.einsum('bhpn,bhn->bhp', state, out_vec)]
    pallas_call x3 -> x2, Pallas kernels: 53.8 us -> 57.9 us  [the longest x1 51.8 us: shards(): pl.pallas_call(functools.partial(mixer_kernel, ntp, ndp), out_shape=(pltp...]
    another operation x9 -> x0, other arithmetic: 3.73 us -> none  [the longest x4 2.1 us: shards(): return (current, jnp.stack(convs), jnp.stack(vec_rows), new_ssm)]
    reduce_sum x8 -> x0, other arithmetic: 2.1 us -> none  [the longest x2 1.49 us: head_step(): jnp.sum(vec_window.astype(jnp.float32) * conv_vec[layer].astype(jnp.float...]
    convert_element_type x3 -> x0, other arithmetic: 2.03 us -> none  [the longest x2 1.31 us: head_step(): (grouped.reshape(local_rows, columns) * out_gain[layer].astype(jnp.float3...]
    mul x7 -> x0, other arithmetic: 1.89 us -> none  [the longest x1 0.79 us: head_step(): grouped.reshape(local_rows, columns) * out_gain[layer].astype(jnp.float32)]
    mul x4 -> x0, local copies, waits for them, and re-layouts: 1.67 us -> none  [the longest x1 0.76 us: head_step(): skip_gain[layer][None, :, None] * values]
where the time goes in v1:
time: 58.8 us; the launch traced here: 58.5 us
  Pallas kernels  57.9 us (98%)
  between operations  0.65 us (1%)
    pallas_call x1, Pallas kernels, shards(): pl.pallas_call(functools.partial(mixer_kernel, ntp, ndp), out_shape=(pltp...  51.8 us
    pallas_call x1, Pallas kernels, shards(): pl.pallas_call(write_kernel, out_shape=tuple((jax.ShapeDtypeStruct(r.shap...  6.06 us

profile of v1, /device:TPU:0, one launch (start us, length us, event | category | flops | bytes accessed | tf_op | source)
XLA Modules:
  0.0 58.5 jit_solution(12906092325321563633)
XLA Ops:
  0.6 51.8 %shard_map.174 = (bf16[8,1024]{1,0:T(8,128)(2,1)S(1)}, bf16[2,3,8,2048]{3,2,1,0:T(8,128)(2,1)S(1)}, bf16[2,2,3,8,512]{4,3,2,1,0:T(8,128)(2,1)S(1)}, f32[2,8,32,64,128]{4,3,2,1,0:T(8,128)S(1)}) custom-call(bf16[8,1024]{1,0:T(8,128)(2,1)} %x_ref.1, bf16[2,1024]{1,0:T(2,128)(2,1)} %gain_hbm.1, bf16[2,1024,128]{2,1,0:T(8,128)(2,1)} %w_step_hbm.1, ...), custom_call_target="tpu_custom_call" | custom-call | tf_op jit(solution)/shard_map/pallas_call | solution.py:460
  52.5 6.1 %shard_map.175 = (bf16[8,1024]{1,0:T(8,128)(2,1)}, bf16[2,3,8,2048]{3,2,1,0:T(8,128)(2,1)}, bf16[2,2,3,8,512]{4,3,2,1,0:T(8,128)(2,1)}, f32[2,8,32,64,128]{4,3,2,1,0:T(8,128)}) custom-call(bf16[8,1024]{1,0:T(8,128)(2,1)S(1)} %get-tuple-element.12.tok, bf16[2,3,8,2048]{3,2,1,0:T(8,128)(2,1)S(1)} %get-tuple-element.13.conv, ...), custom_call_target="tpu_custom_call" | custom-call | tf_op jit(solution)/shard_map/pallas_call | solution.py:478

commit v2 on v1

v2 whole, which is shorter than its diff:
```python
import functools
import types

import jax
import jax.numpy as jnp
from jax import lax
from jax.experimental import pallas as pl
from jax.experimental.pallas import tpu as pltpu
from jax.sharding import PartitionSpec as P

MODEL_WIDTH = 4096
HEAD_DIM = 64
STATE_DIM = 128
LANES = 128
LAYER_COUNT = 2

EPS = 1e-06
F32 = jnp.float32
BF16 = jnp.bfloat16


def remote(src, dst, send_sem, recv_sem, axis, target):
    return pltpu.make_async_remote_copy(
        src_ref=src,
        dst_ref=dst,
        send_sem=send_sem,
        recv_sem=recv_sem,
        device_id={axis: target},
        device_id_type=pl.DeviceIdType.MESH,
    )


def greet(sizes):
    barrier = pltpu.get_barrier_semaphore()
    count = 0
    for axis, n in sizes:
        me = lax.axis_index(axis)
        for k in range(1, n):
            pl.semaphore_signal(
                barrier,
                inc=1,
                device_id={axis: lax.rem(me + k, n)},
                device_id_type=pl.DeviceIdType.MESH,
            )
            count += 1
    pl.semaphore_wait(barrier, count)


def silu(v):
    return v / (1.0 + jnp.exp(-v))


def softplus(v):
    return jnp.maximum(v, 0.0) + jnp.log1p(jnp.exp(-jnp.abs(v)))


def expand(per_head, at, rows):
    per = LANES // HEAD_DIM
    lane = lax.broadcasted_iota(jnp.int32, (rows, LANES), 1)
    out = jnp.broadcast_to(per_head[:, at : at + 1], (rows, LANES))
    for j in range(1, per):
        other = jnp.broadcast_to(per_head[:, at + j : at + j + 1], (rows, LANES))
        out = jnp.where(lane >= j * HEAD_DIM, other, out)
    return out


SEND_KINDS = ("x", "a", "b", "p", "n", "o")


def far_first(me, n):
    low = jnp.asarray(me < (n + 1) // 2, jnp.int32)
    out = []
    for j in range(n - 1):
        up = j + jnp.asarray(j >= me, jnp.int32)
        down = n - 1 - (j + jnp.asarray(j >= n - 1 - me, jnp.int32))
        out.append(low * down + (1 - low) * up)
    return out


def settle(ref, sem):
    pltpu.make_async_copy(ref, ref, sem).wait()


def mixer_kernel(ntp, ndp, names, *refs):
    s = types.SimpleNamespace(**dict(zip(names, refs)))
    outs = refs[len(names) - len(SCRATCH) - (ntp - 1) : len(names) - len(SCRATCH)]
    rows_t, width = s.x.shape
    batch = rows_t * ntp
    rows_d = batch // ndp
    cols = s.w_in.shape[3]
    vcols = s.w_vec.shape[3]
    heads = s.w_step.shape[2]
    local_heads = s.ssm.shape[2]
    groups = vcols // STATE_DIM
    span = cols // groups
    group_heads = local_heads // groups
    block = s.send_p.shape[4]
    blocks = cols // block
    tp = lax.axis_index("tp")
    dp = lax.axis_index("dp")
    far = far_first(dp, ndp)

    def load(src, dst, sem):
        copy = pltpu.make_async_copy(src, dst, sem)
        copy.start()
        return copy

    def load_weights(layer):
        vec = [
            load(s.w_vec_hbm.at[layer, role], s.w_vec.at[layer, role], s.weight_sem.at[layer, role])
            for role in (1, 0)
        ]
        step = load(s.w_step_hbm.at[layer], s.w_step.at[layer], s.weight_sem.at[layer, 2])
        return vec, step, [
            load(s.w_in_hbm.at[layer, role], s.w_in.at[layer, role], s.weight_sem.at[layer, 3 + role])
            for role in (1, 0)
        ]

    def load_rest(layer):
        return (
            load(s.ssm_hbm.at[layer], s.ssm.at[layer], s.weight_sem.at[layer, 5]),
            load(s.w_out_hbm.at[layer], s.w_out.at[layer], s.weight_sem.at[layer, 6]),
        )

    weights = [load_weights(0)]
    smalls = [
        load(getattr(s, name + "_hbm"), getattr(s, name), s.small_sem.at[i])
        for i, name in enumerate(SMALLS)
    ]
    greet((("tp", ntp), ("dp", ndp)))
    for k in range(1, ntp):
        remote(
            s.x, s.landed.at[tp], s.sent.at[0], s.got_x.at[0], "tp", lax.rem(tp + k, ntp)
        ).start()
    s.landed[tp] = s.x[...]
    s.drive_pad[...] = jnp.zeros_like(s.drive_pad)
    s.decay_pad[...] = jnp.zeros_like(s.decay_pad)
    s.outer[...] = jnp.zeros_like(s.outer)
    for copy in smalls:
        copy.wait()
    settle(s.landed.at[pl.ds(0, ntp - 1)], s.got_x.at[0])
    rest = [load_rest(0)]

    def project(layer, rows):
        scale_row = s.gain[...].astype(F32)[layer : layer + 1]
        squares = []
        for i in range(ntp):
            part = rows(i)
            squares.append(jnp.sum(part * part, axis=1, keepdims=True))
            s.lhs_buf[i * rows_t : (i + 1) * rows_t, :] = part * scale_row
        squares = jnp.concatenate(squares, axis=0)
        lhs = s.lhs_buf[...].astype(BF16)
        load_vec, load_step, load_in = weights[layer]

        def put(target, at, acc):
            for p in range(ndp):
                target[p, :, at : at + acc.shape[1]] = acc[p * rows_d : (p + 1) * rows_d].astype(
                    BF16
                )

        def deal(target, landing, kind, got):
            for peer in far:
                remote(
                    target.at[peer], landing.at[dp], s.sent.at[SEND_KINDS.index(kind)], got,
                    "dp", peer,
                ).start()

        load_vec[0].wait()
        put(s.send_a.at[layer], 0, jnp.dot(lhs, s.w_vec[layer, 1], preferred_element_type=F32))
        deal(s.send_a.at[layer], s.land_a.at[layer], "a", s.got_a.at[layer])
        load_step.wait()
        load_vec[1].wait()
        small = jnp.dot(lhs, s.w_step[layer], preferred_element_type=F32)
        small = pltpu.roll(small, lax.rem(heads - tp * local_heads, heads), 1)
        lane = lax.broadcasted_iota(jnp.int32, small.shape, 1)
        small = jnp.where(lane == local_heads, jnp.broadcast_to(squares, small.shape), small)
        put(s.send_b.at[layer], vcols, small)
        put(s.send_b.at[layer], 0, jnp.dot(lhs, s.w_vec[layer, 0], preferred_element_type=F32))
        deal(s.send_b.at[layer], s.land_b.at[layer], "b", s.got_b.at[layer])
        for j, role in enumerate((1, 0)):
            load_in[j].wait()
            for b in range(blocks):
                c = j * blocks + b
                acc = jnp.dot(
                    lhs, s.w_in[layer, role, :, b * block : (b + 1) * block],
                    preferred_element_type=F32,
                )
                put(s.send_p.at[layer, c], 0, acc)
                deal(s.send_p.at[layer, c], s.land_p.at[layer, c], "p", s.got_p.at[layer, c])

    def total(mine, others):
        acc = mine[dp].astype(F32)
        for k in range(1, ndp):
            acc = acc + others[lax.rem(dp + k, ndp)].astype(F32)
        return acc

    def arrived(landing, got):
        settle(landing.at[pl.ds(0, ndp - 1)], got)

    def head_step(layer):
        arrived(s.land_a.at[layer], s.got_a.at[layer])
        arrived(s.land_b.at[layer], s.got_b.at[layer])
        small = total(s.send_b.at[layer], s.land_b.at[layer])
        own_sq = small[:, vcols + local_heads : vcols + local_heads + 1]
        scale = lax.rsqrt(own_sq * (1.0 / MODEL_WIDTH) + EPS)
        taps_v = s.conv_v[layer].astype(F32)
        acts = []
        for role in range(2):
            raw = small[:, 0:vcols] if role == 0 else total(s.send_a.at[layer], s.land_a.at[layer])
            fresh = (raw * scale).astype(BF16)
            acc = fresh.astype(F32) * taps_v[role, 3:4]
            for i in range(3):
                acc = acc + s.vec_s[layer, role, i].astype(F32) * taps_v[role, i : i + 1]
            s.new_vec[layer, role, 0] = s.vec_s[layer, role, 1]
            s.new_vec[layer, role, 1] = s.vec_s[layer, role, 2]
            s.new_vec[layer, role, 2] = fresh
            acts.append(silu(acc))
        in_vec, out_vec = acts
        step = softplus(
            small[:, vcols : vcols + local_heads] * scale + s.bias[layer : layer + 1]
        )
        decay = jnp.exp(-step * jnp.exp(s.decay_log[layer : layer + 1]))
        s.decay_pad[0:rows_d, 0:local_heads] = decay
        s.decay_t[...] = jnp.transpose(s.decay_pad[...])
        rest[layer][0].wait()
        row = lax.broadcasted_iota(jnp.int32, (rows_d, STATE_DIM), 0)
        skips = jnp.broadcast_to(s.skip[layer : layer + 1], (rows_d, local_heads))
        inner = []
        for g in range(groups):
            in_g = in_vec[:, g * STATE_DIM : (g + 1) * STATE_DIM]
            out_g = out_vec[:, g * STATE_DIM : (g + 1) * STATE_DIM]
            inner.append(jnp.sum(in_g * out_g, axis=1, keepdims=True))
            acc = jnp.zeros((rows_d, span), F32)
            for r in range(rows_d):
                mine = jnp.where(row == r, out_g, 0.0)
                state = s.ssm[layer, r, g * group_heads : (g + 1) * group_heads]
                acc = acc + lax.dot_general(
                    mine, state.reshape(span, STATE_DIM), (((1,), (1,)), ((), ())),
                    preferred_element_type=F32,
                )
            s.read[:, g * span : (g + 1) * span] = acc
            high = in_g.astype(BF16).astype(F32)
            for r in range(rows_d):
                at = (r % 2) * STATE_DIM
                lanes = slice(at, at + STATE_DIM)
                mine = jnp.where(row == r, high, 0.0)
                s.outer[g, r // 2, 0:rows_d, lanes] = mine
                s.outer[g, r // 2, rows_d : 2 * rows_d, lanes] = mine
                s.outer[g, r // 2, 2 * rows_d : 3 * rows_d, lanes] = jnp.where(
                    row == r, in_g - high, 0.0
                )
        taps = s.conv_w[layer].astype(F32)
        for b in range(blocks):
            arrived(s.land_p.at[layer, b], s.got_p.at[layer, b])
            cut = slice(b * block, (b + 1) * block)
            fresh = (total(s.send_p.at[layer, b], s.land_p.at[layer, b]) * scale).astype(BF16)
            acc = fresh.astype(F32) * taps[3:4, cut]
            for i in range(3):
                acc = acc + s.conv_s[layer, i, :, cut].astype(F32) * taps[i : i + 1, cut]
            s.new_conv[layer, 0, :, cut] = s.conv_s[layer, 1, :, cut]
            s.new_conv[layer, 1, :, cut] = s.conv_s[layer, 2, :, cut]
            s.new_conv[layer, 2, :, cut] = fresh
            values = silu(acc)
            for at in range(0, block, LANES):
                lane0 = b * block + at
                head = lane0 // HEAD_DIM
                v = values[:, at : at + LANES]
                drive = expand(step, head, rows_d) * v
                lanes = slice(lane0, lane0 + LANES)
                high = drive.astype(BF16).astype(F32)
                s.drive_pad[0:rows_d, lanes] = high
                s.drive_pad[rows_d : 2 * rows_d, lanes] = drive - high
                s.drive_pad[2 * rows_d : 3 * rows_d, lanes] = high
                s.read[:, lanes] = (
                    expand(decay, head, rows_d) * s.read[:, lanes]
                    + drive * inner[lane0 // span]
                    + expand(skips, head, rows_d) * v
                )
        for at in range(0, cols, LANES):
            s.drive_t[at : at + LANES, :] = jnp.transpose(s.drive_pad[:, at : at + LANES])
        gain_row = s.out_gain[...].astype(F32)[layer : layer + 1]
        for b in range(blocks):
            c = blocks + b
            arrived(s.land_p.at[layer, c], s.got_p.at[layer, c])
            fresh = (total(s.send_p.at[layer, c], s.land_p.at[layer, c]) * scale).astype(BF16)
            mixed = s.read[:, b * block : (b + 1) * block] * silu(fresh.astype(F32))
            for at in range(0, block, span):
                cut = slice(b * block + at, b * block + at + span)
                part = mixed[:, at : at + span]
                mean = jnp.mean(part * part, axis=1, keepdims=True)
                s.held[layer, dp, :, cut] = (
                    part * lax.rsqrt(mean + EPS) * gain_row[:, cut]
                ).astype(BF16)
            mine = s.held.at[layer, dp, :, pl.ds(b * block, block)]
            for peer in far:
                remote(
                    mine, mine, s.sent.at[SEND_KINDS.index("n")], s.got_n.at[layer, b], "dp", peer
                ).start()

    def update_state(layer):
        some = min(4, group_heads)

        def some_heads(q, carry):
            first = q * some
            lhs = s.drive_t[pl.ds(pl.multiple_of(first * HEAD_DIM, HEAD_DIM), some * HEAD_DIM), :]
            for pair in range(rows_d // 2):
                added = jnp.dot(
                    lhs, s.outer[first // group_heads, pair], preferred_element_type=F32
                )
                for r in (2 * pair, 2 * pair + 1):
                    at = (r % 2) * STATE_DIM
                    for j in range(some):
                        decay = s.decay_t[pl.ds(first + j, 1), :][:, r : r + 1]
                        s.ssm[layer, r, first + j] = (
                            s.ssm[layer, r, first + j]
                            * jnp.broadcast_to(decay, (HEAD_DIM, STATE_DIM))
                            + added[j * HEAD_DIM : (j + 1) * HEAD_DIM, at : at + STATE_DIM]
                        )
            return carry

        lax.fori_loop(0, local_heads // some, some_heads, 0)

    def gather_out(layer):
        rest[layer][1].wait()
        acc = jnp.zeros((batch, width), F32)
        for b in range(blocks):
            cut = slice(b * block, (b + 1) * block)
            settle(s.held.at[layer, pl.ds(0, ndp - 1), :, pl.ds(b * block, block)], s.got_n.at[layer, b])
            for i in range(ndp):
                s.lhs_out[i * rows_d : (i + 1) * rows_d, cut] = s.held[layer, i, :, cut].astype(F32)
            acc = acc + jnp.dot(
                s.lhs_out[:, cut].astype(BF16), s.w_out[layer, cut, :], preferred_element_type=F32
            )
        return acc

    project(0, lambda i: s.landed[i].astype(F32))
    for layer in range(LAYER_COUNT):
        last = layer == LAYER_COUNT - 1
        if not last:
            weights.append(load_weights(layer + 1))
            rest.append(load_rest(layer + 1))
        head_step(layer)
        update_state(layer)
        acc = gather_out(layer)
        if last:
            for i in range(ntp):
                s.sums[i] = acc[i * rows_t : (i + 1) * rows_t]
            s.base[...] = s.rows[tp].astype(F32) + s.sums[tp]
            for k in range(1, ntp):
                outs[k - 1][...] = s.sums[lax.rem(tp + k, ntp)].astype(BF16)
        else:
            s.part_out[layer] = acc.astype(BF16)
            for k in range(1, ntp):
                remote(
                    s.part_out.at[layer], s.parts_in.at[layer, tp],
                    s.sent.at[SEND_KINDS.index("o")], s.got_o.at[layer],
                    "tp", lax.rem(tp + k, ntp),
                ).start()
            settle(s.parts_in.at[layer, pl.ds(0, ntp - 1)], s.got_o.at[layer])
            s.parts_in[layer, tp] = s.part_out[layer]
            acc = s.parts_in[layer, 0].astype(F32)
            for i in range(1, ntp):
                acc = acc + s.parts_in[layer, i].astype(F32)
            before = s.landed if layer == 0 else s.rows

            def rows(i, before=before, acc=acc):
                part = (before[i].astype(F32) + acc[i * rows_t : (i + 1) * rows_t]).astype(BF16)
                s.rows[i] = part
                return part.astype(F32)

            project(layer + 1, rows)
    settle(s.landed.at[pl.ds(0, ntp - 1)], s.sent.at[0])
    settle(s.send_a.at[:, pl.ds(0, ndp - 1)], s.sent.at[1])
    settle(s.send_b.at[:, pl.ds(0, ndp - 1)], s.sent.at[2])
    settle(s.send_p.at[:, :, pl.ds(0, ndp - 1)], s.sent.at[3])
    settle(s.held.at[:, pl.ds(0, ndp - 1)], s.sent.at[4])
    settle(s.parts_in.at[:, pl.ds(0, ntp - 1)], s.sent.at[5])


def write_kernel(conv, vec, ssm, conv_out, vec_out, ssm_out, sem, ssm_sem):
    layers, rows = ssm.shape[:2]
    for l in range(layers):
        for r in range(rows):
            pltpu.make_async_copy(ssm.at[l, r], ssm_out.at[l, r], ssm_sem).start()
    others = []
    for i, (src, dst) in enumerate(((conv, conv_out), (vec, vec_out))):
        others.append(pltpu.make_async_copy(src, dst, sem.at[i]))
        others[-1].start()
    for copy in others:
        copy.wait()
    pltpu.make_async_copy(ssm, ssm_out, ssm_sem).wait()


VMEM = pl.BlockSpec(memory_space=pltpu.VMEM)
HBM = pl.BlockSpec(memory_space=pl.ANY)


def dma(*shape):
    return pltpu.SemaphoreType.DMA(shape)


SMALLS = (
    "gain", "conv_w", "conv_v", "conv_s", "vec_s", "bias", "decay_log", "skip", "out_gain"
)
INPUTS = ("x", "w_step_hbm", "w_in_hbm", "w_vec_hbm", "w_out_hbm", "ssm_hbm") + tuple(
    name + "_hbm" for name in SMALLS
)
SCRATCH = (
    "w_step", "w_in", "w_vec", "w_out",
) + SMALLS + (
    "landed", "lhs_buf", "send_a", "land_a", "send_b", "land_b", "send_p", "land_p",
    "read", "drive_pad", "drive_t", "outer", "decay_pad", "decay_t",
    "held", "lhs_out", "part_out", "parts_in", "rows", "sums",
    "small_sem", "weight_sem", "sent", "got_x", "got_a", "got_b", "got_p", "got_n", "got_o",
)


def shards(
    ntp, ndp, tokens, w_in, w_vec, w_step, conv_weight, conv_vec, conv_state, vec_state,
    ssm_state, step_bias, decay_log, skip_gain, mix_gain, out_gain, w_out,
):
    rows_t, width = tokens.shape
    layers = w_in.shape[0]
    batch = rows_t * ntp
    rows_d = batch // ndp
    cols, vcols = w_in.shape[3], w_vec.shape[3]
    groups = vcols // STATE_DIM
    block = min(cols, 1024)
    chunks = 2 * cols // block
    conv_rows = jnp.transpose(conv_state, (0, 2, 1, 3))
    vec_rows = jnp.transpose(vec_state, (0, 1, 3, 2, 4))
    smalls = (
        mix_gain, conv_weight, conv_vec, conv_rows, vec_rows, step_bias, decay_log, skip_gain,
        out_gain,
    )
    scratch = [pltpu.VMEM(a.shape, a.dtype) for a in (w_step, w_in, w_vec, w_out) + smalls] + [
        pltpu.VMEM((ntp, rows_t, width), BF16),
        pltpu.VMEM((batch, width), F32),
        pltpu.VMEM((layers, ndp, rows_d, vcols), BF16),
        pltpu.VMEM((layers, ndp, rows_d, vcols), BF16),
        pltpu.VMEM((layers, ndp, rows_d, vcols + LANES), BF16),
        pltpu.VMEM((layers, ndp, rows_d, vcols + LANES), BF16),
        pltpu.VMEM((layers, chunks, ndp, rows_d, block), BF16),
        pltpu.VMEM((layers, chunks, ndp, rows_d, block), BF16),
        pltpu.VMEM((rows_d, cols), F32),
        pltpu.VMEM((LANES, cols), F32),
        pltpu.VMEM((cols, LANES), F32),
        pltpu.VMEM((groups, rows_d // 2, LANES, 2 * STATE_DIM), F32),
        pltpu.VMEM((LANES, LANES), F32),
        pltpu.VMEM((LANES, LANES), F32),
        pltpu.VMEM((layers, ndp, rows_d, cols), BF16),
        pltpu.VMEM((batch, cols), F32),
        pltpu.VMEM((layers - 1, batch, width), BF16),
        pltpu.VMEM((layers - 1, ntp, batch, width), BF16),
        pltpu.VMEM((ntp, rows_t, width), BF16),
        pltpu.VMEM((ntp, rows_t, width), F32),
        dma(len(SMALLS)), dma(layers, 7), dma(6), dma(1), dma(layers), dma(layers),
        dma(layers, chunks), dma(layers, chunks // 2), dma(layers - 1),
    ]
    out_shape = (
        pltpu.VMEM(tokens.shape, F32),
        pltpu.VMEM(conv_rows.shape, BF16),
        pltpu.VMEM(vec_rows.shape, BF16),
        pltpu.VMEM(ssm_state.shape, F32),
    ) + tuple(pltpu.VMEM(tokens.shape, BF16) for _ in range(ntp - 1))
    names = (
        INPUTS + ("base", "new_conv", "new_vec", "ssm")
        + tuple(f"out{k}" for k in range(1, ntp)) + SCRATCH
    )
    base, new_conv, new_vec, new_ssm, *parts = pl.pallas_call(
        functools.partial(mixer_kernel, ntp, ndp, names),
        out_shape=out_shape,
        in_specs=[VMEM] + [HBM] * (len(INPUTS) - 1),
        out_specs=(VMEM,) * len(out_shape),
        scratch_shapes=scratch,
        compiler_params=pltpu.CompilerParams(
            collective_id=0, has_side_effects=True, vmem_limit_bytes=44 << 20
        ),
    )(tokens, w_step, w_in, w_vec, w_out, ssm_state, *smalls)
    parts = [
        lax.ppermute(part, "tp", [(i, (i + k) % ntp) for i in range(ntp)])
        for k, part in enumerate(parts, 1)
    ]
    results = (new_conv, new_vec, new_ssm)
    new_conv, new_vec, new_ssm = pl.pallas_call(
        write_kernel,
        out_shape=tuple(jax.ShapeDtypeStruct(r.shape, r.dtype) for r in results),
        in_specs=[VMEM] * 3,
        out_specs=(HBM,) * 3,
        scratch_shapes=[dma(2), pltpu.SemaphoreType.DMA],
        compiler_params=pltpu.CompilerParams(vmem_limit_bytes=8 << 20),
        cost_estimate=pl.CostEstimate(
            flops=40_000_000, bytes_accessed=2 * new_ssm.size * 4, transcendentals=0
        ),
    )(*results)
    total = base
    for part in parts:
        total = total + part.astype(F32)
    return (
        total.astype(BF16),
        jnp.transpose(new_conv, (0, 2, 1, 3)),
        jnp.transpose(new_vec, (0, 1, 3, 2, 4)),
        new_ssm,
    )


def solution(mesh):
    placed = (
        P(("grp", "tp"), "dp"),
        P(None, None, "dp", "tp"),
        P(None, None, "dp", "tp"),
        P(None, "dp", None),
        P(None, None, "tp"),
        P(None, None, None, "tp"),
        P(None, ("grp", "dp"), None, "tp"),
        P(None, None, ("grp", "dp"), None, "tp"),
        P(None, ("grp", "dp"), "tp", None, None),
        P(None, "tp"),
        P(None, "tp"),
        P(None, "tp"),
        P(None, "dp"),
        P(None, "tp"),
        P(None, "tp", "dp"),
    )
    return jax.shard_map(
        functools.partial(shards, mesh.shape["tp"], mesh.shape["dp"]),
        mesh=mesh,
        in_specs=placed,
        out_specs=(
            P(("grp", "tp"), "dp"),
            P(None, ("grp", "dp"), None, "tp"),
            P(None, None, ("grp", "dp"), None, "tp"),
            P(None, ("grp", "dp"), "tp", None, None),
        ),
        check_vma=False,
    )
```

time: 58.8 us -> 52.4 us (0.89)
  Pallas kernels: 57.9 us -> 47.9 us
  starting transfers between devices: 0 us -> 3.03 us
  other arithmetic: 0 us -> 0.62 us
    pallas_call x1, Pallas kernels: 51.8 us -> 42 us  [shards(): pl.pallas_call(functools.partial(mixer_kernel, ntp, ndp, names), out_shap...]
    ppermute x0 -> x3, starting transfers between devices: none -> 3.03 us  [shards(): lax.ppermute(part, 'tp', [(i, (i + k) % ntp) for i in range(ntp)])]
    convert_element_type x0 -> x1, other arithmetic: none -> 0.62 us  [shards(): total.astype(BF16)]
  transfers between devices with their start and end apart: 0 -> 3, of which waited for: 0 -> 0; matrix products, arithmetic and copies ran while one was open for 0% -> 0% of each run, Pallas kernels for 0% -> 11%
where the time goes in v2:
time: 52.4 us; the launch traced here: 52.2 us
  Pallas kernels  47.9 us (91%)
  starting transfers between devices  3.03 us (6%)
  between operations  0.69 us (1%)
  other arithmetic  0.62 us (1%)
    pallas_call x1, Pallas kernels, shards(): pl.pallas_call(functools.partial(mixer_kernel, ntp, ndp, names), out_shap...  42 us
    pallas_call x1, Pallas kernels, shards(): pl.pallas_call(write_kernel, out_shape=tuple((jax.ShapeDtypeStruct(r.shap...  5.9 us
    ppermute x3, starting transfers between devices, shards(): lax.ppermute(part, 'tp', [(i, (i + k) % ntp) for i in range(ntp)])  3.03 us
  transfers between devices with their start and end apart: 3, of which 0 were waited for; matrix products, arithmetic and copies ran while one was open for 0% of the time, Pallas kernels for 11%

profile of v2, /device:TPU:0, one launch (start us, length us, event | category | flops | bytes accessed | tf_op | source)
XLA Modules:
  0.0 52.2 jit_solution(15839282977322923586)
XLA Ops:
  0.6 42.0 %shard_map.174 = (f32[8,1024]{1,0:T(8,128)S(1)}, bf16[2,3,8,2048]{3,2,1,0:T(8,128)(2,1)S(1)}, bf16[2,2,3,8,512]{4,3,2,1,0:T(8,128)(2,1)S(1)}, f32[2,8,32,64,128]...) custom-call(bf16[8,1024]{1,0:T(8,128)(2,1)} %refs_0_.1, ...), custom_call_target="tpu_custom_call" | custom-call | tf_op jit(solution)/shard_map/pallas_call | solution.py:470
  42.6 0.1 collective-permute-start
  42.7 1.6 %collective-permute-start.1 = (bf16[8,1024]{1,0:T(8,128)(2,1)S(1)}, bf16[8,1024]{1,0:T(8,128)(2,1)S(1)}, u32[]{:S(2)}, u32[]{:S(2)}) collective-permute-start(bf16[8,1024]{1,0:T(8,128)(2,1)S(1)} %get-tuple-element.16), channel_id=1, source_target_pairs={{0,8},{4,12},{8,0},{12,4},{1,9},{5,13},{9,1},{13,5},{2,10},{6,14},... | collective-permute-start | bytes 49160 | tf_op jit(solution)/shard_map/ppermute | solution.py:481
  44.2 1.4 %collective-permute-start.2 = (bf16[8,1024]{1,0:T(8,128)(2,1)S(1)}, bf16[8,1024]{1,0:T(8,128)(2,1)S(1)}, u32[]{:S(2)}, u32[]{:S(2)}) collective-permute-start(bf16[8,1024]{1,0:T(8,128)(2,1)S(1)} %get-tuple-element.17), channel_id=1, source_target_pairs={{0,12},{4,0},{8,4},{12,8},{1,13},{5,1},{9,5},{13,9},{2,14},{6,2},{... | collective-permute-start | bytes 49160 | tf_op jit(solution)/shard_map/ppermute | solution.py:481
  45.6 5.9 %shard_map.175 = (bf16[2,3,8,2048]{3,2,1,0:T(8,128)(2,1)}, bf16[2,2,3,8,512]{4,3,2,1,0:T(8,128)(2,1)}, f32[2,8,32,64,128]{4,3,2,1,0:T(8,128)}) custom-call(bf16[2,3,8,2048]{3,2,1,0:T(8,128)(2,1)S(1)} %get-tuple-element.18.conv, bf16[2,2,3,8,512]{4,3,2,1,0:T(8,128)(2,1)S(1)} %get-tuple-element.19.vec, f32[2,8,32,64,128]{4,3,2,1,0:T(8,128)S(1)} %get-tuple-element.20.ssm), custom_call_target="tpu_custom_call" | custom-call | flops 40000000 | bytes 33554432 | tf_op jit(solution)/shard_map/pallas_call | solution.py:485
  51.5 0.0 collective-permute-done
  51.6 0.0 collective-permute-done.1
  51.6 0.0 collective-permute-done.2
  51.6 0.6 %add_convert_fusion = bf16[8,1024]{1,0:T(8,128)(2,1)} fusion(bf16[8,1024]{1,0:T(8,128)(2,1)S(1)} %collective-permute-done.2, bf16[8,1024]{1,0:T(8,128)(2,1)S(1)} %collective-permute-done.1, f32[8,1024]{1,0:T(8,128)S(1)} %get-tuple-element.14, bf16[8,1024]{1,0:T(8,128)(2,1)S(1)} %collective-permute-done), kind=kLoop, calls=%fused_computation | loop fusion | flops 57344 | bytes 98304 | tf_op jit(solution)/shard_map/convert_element_type | solution.py:500
Async XLA Ops:
  42.6 9.0 %collective-permute-start = (bf16[8,1024]{1,0:T(8,128)(2,1)S(1)}, bf16[8,1024]{1,0:T(8,128)(2,1)S(1)}, u32[]{:S(2)}, u32[]{:S(2)}) collective-permute-start(bf16[8,1024]{1,0:T(8,128)(2,1)S(1)} %get-tuple-element.15), channel_id=1, source_target_pairs={{0,4},{4,8},{8,12},{12,0},{1,5},{5,9},{9,13},{13,1},{2,6},{6,10},{... | collective-permute-start | bytes 49160 | tf_op jit(solution)/shard_map/ppermute | solution.py:481
  42.7 8.9 %collective-permute-start.1 = (bf16[8,1024]{1,0:T(8,128)(2,1)S(1)}, bf16[8,1024]{1,0:T(8,128)(2,1)S(1)}, u32[]{:S(2)}, u32[]{:S(2)}) collective-permute-start(bf16[8,1024]{1,0:T(8,128)(2,1)S(1)} %get-tuple-element.16), channel_id=1, source_target_pairs={{0,8},{4,12},{8,0},{12,4},{1,9},{5,13},{9,1},{13,5},{2,10},{6,14},... | collective-permute-start | bytes 49160 | tf_op jit(solution)/shard_map/ppermute | solution.py:481
  44.2 7.3 %collective-permute-start.2 = (bf16[8,1024]{1,0:T(8,128)(2,1)S(1)}, bf16[8,1024]{1,0:T(8,128)(2,1)S(1)}, u32[]{:S(2)}, u32[]{:S(2)}) collective-permute-start(bf16[8,1024]{1,0:T(8,128)(2,1)S(1)} %get-tuple-element.17), channel_id=1, source_target_pairs={{0,12},{4,0},{8,4},{12,8},{1,13},{5,1},{9,5},{13,9},{2,14},{6,2},{... | collective-permute-start | bytes 49160 | tf_op jit(solution)/shard_map/ppermute | solution.py:481

commit v3 on v2

--- a/solution.py
+++ b/solution.py
@@ -64,7 +64,7 @@
     return out
 
 
-SEND_KINDS = ("x", "a", "b", "p", "n", "o")
+SEND_KINDS = ("x", "a", "b", "p", "n", "o", "f")
 
 
 def far_first(me, n):
@@ -83,8 +83,7 @@
 
 def mixer_kernel(ntp, ndp, names, *refs):
     s = types.SimpleNamespace(**dict(zip(names, refs)))
-    outs = refs[len(names) - len(SCRATCH) - (ntp - 1) : len(names) - len(SCRATCH)]
-    rows_t, width = s.x.shape
+    rows_t, width = s.tokens.shape
     batch = rows_t * ntp
     rows_d = batch // ndp
     cols = s.w_in.shape[3]
@@ -99,6 +98,10 @@
     tp = lax.axis_index("tp")
     dp = lax.axis_index("dp")
     far = far_first(dp, ndp)
+    relay = ndp == 4
+    at_end = jnp.logical_or(dp == 0, dp == ndp - 1)
+    inside = jnp.logical_not(at_end)
+    across = ndp - 1 - dp
 
     def load(src, dst, sem):
         copy = pltpu.make_async_copy(src, dst, sem)
@@ -122,24 +125,55 @@
             load(s.w_out_hbm.at[layer], s.w_out.at[layer], s.weight_sem.at[layer, 6]),
         )
 
+    own = load(s.x_hbm, s.landed.at[tp], s.own_sem.at[0])
     weights = [load_weights(0)]
     smalls = [
         load(getattr(s, name + "_hbm"), getattr(s, name), s.small_sem.at[i])
         for i, name in enumerate(SMALLS)
     ]
     greet((("tp", ntp), ("dp", ndp)))
+    own.wait()
     for k in range(1, ntp):
         remote(
-            s.x, s.landed.at[tp], s.sent.at[0], s.got_x.at[0], "tp", lax.rem(tp + k, ntp)
+            s.landed.at[tp], s.landed.at[tp], s.sent.at[0], s.got_x.at[0],
+            "tp", lax.rem(tp + k, ntp),
         ).start()
-    s.landed[tp] = s.x[...]
     s.drive_pad[...] = jnp.zeros_like(s.drive_pad)
     s.decay_pad[...] = jnp.zeros_like(s.decay_pad)
     s.outer[...] = jnp.zeros_like(s.outer)
+    if relay:
+        @pl.when(at_end)
+        def _():
+            for layer in range(LAYER_COUNT):
+                for c in range(2 * blocks - 1):
+                    s.land_p[layer, c, across] = jnp.zeros((rows_d, block), BF16)
+
     for copy in smalls:
         copy.wait()
     settle(s.landed.at[pl.ds(0, ntp - 1)], s.got_x.at[0])
     rest = [load_rest(0)]
+
+    def send_part(layer, c, peer):
+        remote(
+            s.send_p.at[layer, c, peer], s.land_p.at[layer, c, dp],
+            s.sent.at[SEND_KINDS.index("p")], s.got_p.at[layer, c], "dp", peer,
+        ).start()
+
+    def deal_relayed(layer, c):
+        @pl.when(at_end)
+        def _():
+            near = jnp.where(dp == 0, 1, ndp - 2)
+            remote(
+                s.send_p.at[layer, c, across], s.land_r.at[layer, c],
+                s.sent.at[SEND_KINDS.index("p")], s.got_r.at[layer, c], "dp", near,
+            ).start()
+            send_part(layer, c, ndp - 1 - near)
+            send_part(layer, c, near)
+
+        @pl.when(inside)
+        def _():
+            send_part(layer, c, across)
+            send_part(layer, c, (dp - 1) * 3)
 
     def project(layer, rows):
         scale_row = s.gain[...].astype(F32)[layer : layer + 1]
@@ -186,7 +220,21 @@
                     preferred_element_type=F32,
                 )
                 put(s.send_p.at[layer, c], 0, acc)
-                deal(s.send_p.at[layer, c], s.land_p.at[layer, c], "p", s.got_p.at[layer, c])
+                if relay and c < 2 * blocks - 1:
+                    deal_relayed(layer, c)
+                else:
+                    deal(s.send_p.at[layer, c], s.land_p.at[layer, c], "p", s.got_p.at[layer, c])
+        if relay:
+            @pl.when(inside)
+            def _():
+                end = (dp - 1) * 3
+                other = 3 - end
+                for c in range(2 * blocks - 1):
+                    settle(s.land_r.at[layer, c], s.got_r.at[layer, c])
+                    s.send_p[layer, c, other] = (
+                        s.send_p[layer, c, other].astype(F32) + s.land_r[layer, c].astype(F32)
+                    ).astype(BF16)
+                    send_part(layer, c, other)
 
     def total(mine, others):
         acc = mine[dp].astype(F32)
@@ -196,6 +244,18 @@
 
     def arrived(landing, got):
         settle(landing.at[pl.ds(0, ndp - 1)], got)
+
+    def arrived_part(layer, c):
+        if relay and c < 2 * blocks - 1:
+            @pl.when(at_end)
+            def _():
+                settle(s.land_p.at[layer, c, pl.ds(0, ndp - 2)], s.got_p.at[layer, c])
+
+            @pl.when(inside)
+            def _():
+                settle(s.land_p.at[layer, c, pl.ds(0, ndp - 1)], s.got_p.at[layer, c])
+        else:
+            arrived(s.land_p.at[layer, c], s.got_p.at[layer, c])
 
     def head_step(layer):
         arrived(s.land_a.at[layer], s.got_a.at[layer])
@@ -251,7 +311,7 @@
                 )
         taps = s.conv_w[layer].astype(F32)
         for b in range(blocks):
-            arrived(s.land_p.at[layer, b], s.got_p.at[layer, b])
+            arrived_part(layer, b)
             cut = slice(b * block, (b + 1) * block)
             fresh = (total(s.send_p.at[layer, b], s.land_p.at[layer, b]) * scale).astype(BF16)
             acc = fresh.astype(F32) * taps[3:4, cut]
@@ -281,7 +341,7 @@
         gain_row = s.out_gain[...].astype(F32)[layer : layer + 1]
         for b in range(blocks):
             c = blocks + b
-            arrived(s.land_p.at[layer, c], s.got_p.at[layer, c])
+            arrived_part(layer, c)
             fresh = (total(s.send_p.at[layer, c], s.land_p.at[layer, c]) * scale).astype(BF16)
             mixed = s.read[:, b * block : (b + 1) * block] * silu(fresh.astype(F32))
             for at in range(0, block, span):
@@ -320,18 +380,22 @@
 
         lax.fori_loop(0, local_heads // some, some_heads, 0)
 
-    def gather_out(layer):
+    def gather_out(layer, emit):
         rest[layer][1].wait()
-        acc = jnp.zeros((batch, width), F32)
+        half = width // 2
+        accs = [jnp.zeros((batch, half), F32)] * 2
         for b in range(blocks):
             cut = slice(b * block, (b + 1) * block)
             settle(s.held.at[layer, pl.ds(0, ndp - 1), :, pl.ds(b * block, block)], s.got_n.at[layer, b])
             for i in range(ndp):
                 s.lhs_out[i * rows_d : (i + 1) * rows_d, cut] = s.held[layer, i, :, cut].astype(F32)
-            acc = acc + jnp.dot(
-                s.lhs_out[:, cut].astype(BF16), s.w_out[layer, cut, :], preferred_element_type=F32
-            )
-        return acc
+            lhs = s.lhs_out[:, cut].astype(BF16)
+            for h in range(2):
+                accs[h] = accs[h] + jnp.dot(
+                    lhs, s.w_out[layer, cut, h * half : (h + 1) * half], preferred_element_type=F32
+                )
+                if b == blocks - 1:
+                    emit(h, accs[h])
 
     project(0, lambda i: s.landed[i].astype(F32))
     for layer in range(LAYER_COUNT):
@@ -341,26 +405,41 @@
             rest.append(load_rest(layer + 1))
         head_step(layer)
         update_state(layer)
-        acc = gather_out(layer)
+        half = width // 2
+
+        def emit(h, acc, layer=layer, last=last):
+            kind = s.sent.at[SEND_KINDS.index("f" if last else "o")]
+            got = (s.got_f if last else s.got_o).at[0 if last else layer, h]
+            if last:
+                for i in range(ntp):
+                    s.send_f[h, i] = acc[i * rows_t : (i + 1) * rows_t].astype(BF16)
+            else:
+                s.parts[layer, h, tp] = acc.astype(BF16)
+            for k in range(1, ntp):
+                peer = lax.rem(tp + k, ntp)
+                src = s.send_f.at[h, peer] if last else s.parts.at[layer, h, tp]
+                dst = s.land_f.at[h, tp] if last else src
+                remote(src, dst, kind, got, "tp", peer).start()
+
+        gather_out(layer, emit)
         if last:
-            for i in range(ntp):
-                s.sums[i] = acc[i * rows_t : (i + 1) * rows_t]
-            s.base[...] = s.rows[tp].astype(F32) + s.sums[tp]
-            for k in range(1, ntp):
-                outs[k - 1][...] = s.sums[lax.rem(tp + k, ntp)].astype(BF16)
+            for h in range(2):
+                cut = slice(h * half, (h + 1) * half)
+                settle(s.land_f.at[h, pl.ds(0, ntp - 1)], s.got_f.at[0, h])
+                s.land_f[h, tp] = s.send_f[h, tp]
+                acc = s.rows[tp, :, cut].astype(F32)
+                for i in range(ntp):
+                    acc = acc + s.land_f[h, i].astype(F32)
+                s.tokens[:, cut] = acc.astype(BF16)
         else:
-            s.part_out[layer] = acc.astype(BF16)
-            for k in range(1, ntp):
-                remote(
-                    s.part_out.at[layer], s.parts_in.at[layer, tp],
-                    s.sent.at[SEND_KINDS.index("o")], s.got_o.at[layer],
-                    "tp", lax.rem(tp + k, ntp),
-                ).start()
-            settle(s.parts_in.at[layer, pl.ds(0, ntp - 1)], s.got_o.at[layer])
-            s.parts_in[layer, tp] = s.part_out[layer]
-            acc = s.parts_in[layer, 0].astype(F32)
-            for i in range(1, ntp):
-                acc = acc + s.parts_in[layer, i].astype(F32)
+            accs = []
+            for h in range(2):
+                settle(s.parts.at[layer, h, pl.ds(0, ntp - 1)], s.got_o.at[layer, h])
+                acc = s.parts[layer, h, 0].astype(F32)
+                for i in range(1, ntp):
+                    acc = acc + s.parts[layer, h, i].astype(F32)
+                accs.append(acc)
+            acc = jnp.concatenate(accs, axis=1)
             before = s.landed if layer == 0 else s.rows
 
             def rows(i, before=before, acc=acc):
@@ -374,16 +453,17 @@
     settle(s.send_b.at[:, pl.ds(0, ndp - 1)], s.sent.at[2])
     settle(s.send_p.at[:, :, pl.ds(0, ndp - 1)], s.sent.at[3])
     settle(s.held.at[:, pl.ds(0, ndp - 1)], s.sent.at[4])
-    settle(s.parts_in.at[:, pl.ds(0, ntp - 1)], s.sent.at[5])
-
-
-def write_kernel(conv, vec, ssm, conv_out, vec_out, ssm_out, sem, ssm_sem):
+    settle(s.parts.at[:, :, pl.ds(0, ntp - 1)], s.sent.at[5])
+    settle(s.land_f.at[:, pl.ds(0, ntp - 1)], s.sent.at[6])
+
+
+def write_kernel(tok, conv, vec, ssm, tok_out, conv_out, vec_out, ssm_out, sem, ssm_sem):
     layers, rows = ssm.shape[:2]
     for l in range(layers):
         for r in range(rows):
             pltpu.make_async_copy(ssm.at[l, r], ssm_out.at[l, r], ssm_sem).start()
     others = []
-    for i, (src, dst) in enumerate(((conv, conv_out), (vec, vec_out))):
+    for i, (src, dst) in enumerate(((tok, tok_out), (conv, conv_out), (vec, vec_out))):
         others.append(pltpu.make_async_copy(src, dst, sem.at[i]))
         others[-1].start()
     for copy in others:
@@ -402,7 +482,7 @@
 SMALLS = (
     "gain", "conv_w", "conv_v", "conv_s", "vec_s", "bias", "decay_log", "skip", "out_gain"
 )
-INPUTS = ("x", "w_step_hbm", "w_in_hbm", "w_vec_hbm", "w_out_hbm", "ssm_hbm") + tuple(
+INPUTS = ("x_hbm", "w_step_hbm", "w_in_hbm", "w_vec_hbm", "w_out_hbm", "ssm_hbm") + tuple(
     name + "_hbm" for name in SMALLS
 )
 SCRATCH = (
@@ -410,8 +490,9 @@
 ) + SMALLS + (
     "landed", "lhs_buf", "send_a", "land_a", "send_b", "land_b", "send_p", "land_p",
     "read", "drive_pad", "drive_t", "outer", "decay_pad", "decay_t",
-    "held", "lhs_out", "part_out", "parts_in", "rows", "sums",
-    "small_sem", "weight_sem", "sent", "got_x", "got_a", "got_b", "got_p", "got_n", "got_o",
+    "held", "lhs_out", "parts", "rows", "send_f", "land_f", "land_r",
+    "small_sem", "weight_sem", "own_sem", "sent", "got_x", "got_a", "got_b", "got_p", "got_r",
+    "got_n", "got_o", "got_f",
 )
 
 
@@ -450,54 +531,42 @@
         pltpu.VMEM((LANES, LANES), F32),
         pltpu.VMEM((layers, ndp, rows_d, cols), BF16),
         pltpu.VMEM((batch, cols), F32),
-        pltpu.VMEM((layers - 1, batch, width), BF16),
-        pltpu.VMEM((layers - 1, ntp, batch, width), BF16),
+        pltpu.VMEM((layers - 1, 2, ntp, batch, width // 2), BF16),
         pltpu.VMEM((ntp, rows_t, width), BF16),
-        pltpu.VMEM((ntp, rows_t, width), F32),
-        dma(len(SMALLS)), dma(layers, 7), dma(6), dma(1), dma(layers), dma(layers),
-        dma(layers, chunks), dma(layers, chunks // 2), dma(layers - 1),
+        pltpu.VMEM((2, ntp, rows_t, width // 2), BF16),
+        pltpu.VMEM((2, ntp, rows_t, width // 2), BF16),
+        pltpu.VMEM((layers, chunks - 1, rows_d, block), BF16),
+        dma(len(SMALLS)), dma(layers, 7), dma(1), dma(len(SEND_KINDS)), dma(1), dma(layers),
+        dma(layers), dma(layers, chunks), dma(layers, chunks - 1), dma(layers, chunks // 2),
+        dma(layers - 1, 2), dma(1, 2),
     ]
     out_shape = (
-        pltpu.VMEM(tokens.shape, F32),
+        pltpu.VMEM(tokens.shape, BF16),
         pltpu.VMEM(conv_rows.shape, BF16),
         pltpu.VMEM(vec_rows.shape, BF16),
         pltpu.VMEM(ssm_state.shape, F32),
-    ) + tuple(pltpu.VMEM(tokens.shape, BF16) for _ in range(ntp - 1))
-    names = (
-        INPUTS + ("base", "new_conv", "new_vec", "ssm")
-        + tuple(f"out{k}" for k in range(1, ntp)) + SCRATCH
     )
-    base, new_conv, new_vec, new_ssm, *parts = pl.pallas_call(
+    names = INPUTS + ("tokens", "new_conv", "new_vec", "ssm") + SCRATCH
+    results = pl.pallas_call(
         functools.partial(mixer_kernel, ntp, ndp, names),
         out_shape=out_shape,
-        in_specs=[VMEM] + [HBM] * (len(INPUTS) - 1),
+        in_specs=[HBM] * len(INPUTS),
         out_specs=(VMEM,) * len(out_shape),
         scratch_shapes=scratch,
         compiler_params=pltpu.CompilerParams(
             collective_id=0, has_side_effects=True, vmem_limit_bytes=44 << 20
         ),
     )(tokens, w_step, w_in, w_vec, w_out, ssm_state, *smalls)
-    parts = [
-        lax.ppermute(part, "tp", [(i, (i + k) % ntp) for i in range(ntp)])
-        for k, part in enumerate(parts, 1)
-    ]
-    results = (new_conv, new_vec, new_ssm)
-    new_conv, new_vec, new_ssm = pl.pallas_call(
+    new_tokens, new_conv, new_vec, new_ssm = pl.pallas_call(
         write_kernel,
         out_shape=tuple(jax.ShapeDtypeStruct(r.shape, r.dtype) for r in results),
-        in_specs=[VMEM] * 3,
-        out_specs=(HBM,) * 3,
-        scratch_shapes=[dma(2), pltpu.SemaphoreType.DMA],
+        in_specs=[VMEM] * 4,
+        out_specs=(HBM,) * 4,
+        scratch_shapes=[dma(3), pltpu.SemaphoreType.DMA],
         compiler_params=pltpu.CompilerParams(vmem_limit_bytes=8 << 20),
-        cost_estimate=pl.CostEstimate(
-            flops=40_000_000, bytes_accessed=2 * new_ssm.size * 4, transcendentals=0
-        ),
     )(*results)
-    total = base
-    for part in parts:
-        total = total + part.astype(F32)
     return (
-        total.astype(BF16),
+        new_tokens,
         jnp.transpose(new_conv, (0, 2, 1, 3)),
         jnp.transpose(new_vec, (0, 1, 3, 2, 4)),
         new_ssm,

time: 52.4 us -> 52.7 us (level)
  Pallas kernels: 47.9 us -> 51.9 us
  starting transfers between devices: 3.03 us -> 0 us
  other arithmetic: 0.62 us -> 0 us
    pallas_call x1, Pallas kernels: 42 us -> 46 us  [shards(): pl.pallas_call(functools.partial(mixer_kernel, ntp, ndp, names), out_shap...]
    ppermute x3 -> x0, starting transfers between devices: 3.03 us -> none  [shards(): lax.ppermute(part, 'tp', [(i, (i + k) % ntp) for i in range(ntp)])]
    convert_element_type x1 -> x0, other arithmetic: 0.62 us -> none  [shards(): total.astype(BF16)]
  transfers between devices with their start and end apart: 3 -> 0, of which waited for: 0 -> 0; matrix products, arithmetic and copies ran while one was open for 0% -> 0% of each run, Pallas kernels for 11% -> 0%
where the time goes in v3:
time: 52.7 us; the launch traced here: 52.6 us
  Pallas kernels  51.9 us (98%)
  between operations  0.65 us (1%)
    pallas_call x1, Pallas kernels, shards(): pl.pallas_call(functools.partial(mixer_kernel, ntp, ndp, names), out_shap...  46 us
    pallas_call x1, Pallas kernels, shards(): pl.pallas_call(write_kernel, out_shape=tuple((jax.ShapeDtypeStruct(r.shap...  5.92 us

profile of v3, /device:TPU:0, one launch (start us, length us, event | category | flops | bytes accessed | tf_op | source)
XLA Modules:
  0.0 52.6 jit_solution(16910304004002310446)
XLA Ops:
  0.6 46.0 %shard_map.174 = (bf16[8,1024]{1,0:T(8,128)(2,1)S(1)}, bf16[2,3,8,2048]{3,2,1,0:T(8,128)(2,1)S(1)}, bf16[2,2,3,8,512]{4,3,2,1,0:T(8,128)(2,1)S(1)}, f32[2,8,32,64,128]{4,3,2,1,0:T(8,128)S(1)}) custom-call(bf16[8,1024]{1,0:T(8,128)(2,1)} %refs_0_.1, bf16[2,1024,128]{2,1,0:T(8,128)(2,1)} %refs_1_.1, bf16[2,2,1024,2048]{3,2,1,0:T(8,128)(2,1)} %refs_2_.1, ...), custom_call_target="tpu_custom_call" | custom-call | tf_op jit(solution)/shard_map/pallas_call | solution.py:550
  46.6 5.9 %shard_map.175 = (bf16[8,1024]{1,0:T(8,128)(2,1)}, bf16[2,3,8,2048]{3,2,1,0:T(8,128)(2,1)}, bf16[2,2,3,8,512]{4,3,2,1,0:T(8,128)(2,1)}, f32[2,8,32,64,128]{4,3,2,1,0:T(8,128)}) custom-call(bf16[8,1024]{1,0:T(8,128)(2,1)S(1)} %get-tuple-element.12.tok, bf16[2,3,8,2048]{3,2,1,0:T(8,128)(2,1)S(1)} %get-tuple-element.13.conv, ...), custom_call_target="tpu_custom_call" | custom-call | tf_op jit(solution)/shard_map/pallas_call | solution.py:560

commit v4 on v3

--- a/solution.py
+++ b/solution.py
@@ -30,20 +30,57 @@
     )
 
 
-def greet(sizes):
+def call_out(ntp, ndp):
     barrier = pltpu.get_barrier_semaphore()
-    count = 0
-    for axis, n in sizes:
-        me = lax.axis_index(axis)
-        for k in range(1, n):
-            pl.semaphore_signal(
-                barrier,
-                inc=1,
-                device_id={axis: lax.rem(me + k, n)},
-                device_id_type=pl.DeviceIdType.MESH,
-            )
-            count += 1
-    pl.semaphore_wait(barrier, count)
+    tp, dp = lax.axis_index("tp"), lax.axis_index("dp")
+
+    def call(axis, target):
+        pl.semaphore_signal(
+            barrier, inc=1, device_id={axis: target}, device_id_type=pl.DeviceIdType.MESH
+        )
+
+    @pl.when(dp > 0)
+    def _():
+        call("dp", dp - 1)
+
+    @pl.when(dp < ndp - 1)
+    def _():
+        call("dp", dp + 1)
+
+    for k in range(1, ntp):
+        call("tp", lax.rem(tp + k, ntp))
+    return barrier, ntp - 1 + jnp.asarray(dp > 0, jnp.int32) + jnp.asarray(dp < ndp - 1, jnp.int32)
+
+
+def pass_word(ndp, know):
+    dp = lax.axis_index("dp")
+
+    def tell(side, target):
+        pl.semaphore_signal(
+            know.at[side], inc=1, device_id={"dp": target}, device_id_type=pl.DeviceIdType.MESH
+        )
+
+    @pl.when(jnp.logical_and(dp > 0, dp < ndp - 1))
+    def _():
+        tell(0, dp - 1)
+        tell(1, dp + 1)
+
+    for t in range(ndp - 2):
+        @pl.when(dp < ndp - 2 - t)
+        def _():
+            pl.semaphore_wait(know.at[0], 1)
+
+            @pl.when(dp > 0)
+            def _():
+                tell(0, dp - 1)
+
+        @pl.when(dp > 1 + t)
+        def _():
+            pl.semaphore_wait(know.at[1], 1)
+
+            @pl.when(dp < ndp - 1)
+            def _():
+                tell(1, dp + 1)
 
 
 def silu(v):
@@ -125,14 +162,14 @@
             load(s.w_out_hbm.at[layer], s.w_out.at[layer], s.weight_sem.at[layer, 6]),
         )
 
-    own = load(s.x_hbm, s.landed.at[tp], s.own_sem.at[0])
+    barrier, callers = call_out(ntp, ndp)
+    load(s.x_hbm, s.landed.at[tp], s.own_sem.at[0]).wait()
     weights = [load_weights(0)]
     smalls = [
         load(getattr(s, name + "_hbm"), getattr(s, name), s.small_sem.at[i])
         for i, name in enumerate(SMALLS)
     ]
-    greet((("tp", ntp), ("dp", ndp)))
-    own.wait()
+    pl.semaphore_wait(barrier, callers)
     for k in range(1, ntp):
         remote(
             s.landed.at[tp], s.landed.at[tp], s.sent.at[0], s.got_x.at[0],
@@ -148,6 +185,7 @@
                 for c in range(2 * blocks - 1):
                     s.land_p[layer, c, across] = jnp.zeros((rows_d, block), BF16)
 
+    pass_word(ndp, s.know)
     for copy in smalls:
         copy.wait()
     settle(s.landed.at[pl.ds(0, ntp - 1)], s.got_x.at[0])
@@ -159,21 +197,43 @@
             s.sent.at[SEND_KINDS.index("p")], s.got_p.at[layer, c], "dp", peer,
         ).start()
 
+    near = jnp.where(dp == 0, 1, ndp - 2)
+    middle = ndp - 1 - near
+    side = (dp - 1) * 3
+
     def deal_relayed(layer, c):
+        final = c == 2 * blocks - 1
+
         @pl.when(at_end)
         def _():
-            near = jnp.where(dp == 0, 1, ndp - 2)
-            remote(
-                s.send_p.at[layer, c, across], s.land_r.at[layer, c],
-                s.sent.at[SEND_KINDS.index("p")], s.got_r.at[layer, c], "dp", near,
-            ).start()
-            send_part(layer, c, ndp - 1 - near)
-            send_part(layer, c, near)
+            if not final:
+                remote(
+                    s.send_p.at[layer, c, across], s.land_r.at[layer, c],
+                    s.sent.at[SEND_KINDS.index("p")], s.got_r.at[layer, c], "dp", near,
+                ).start()
+            else:
+                for e in range(c):
+                    send_part(layer, e, middle)
+                send_part(layer, c, across)
+                send_part(layer, c, middle)
+                for e in range(c + 1):
+                    send_part(layer, e, near)
 
         @pl.when(inside)
         def _():
-            send_part(layer, c, across)
-            send_part(layer, c, (dp - 1) * 3)
+            send_part(layer, c, side)
+            if not final:
+                send_part(layer, c, across)
+            else:
+                other = 3 - side
+                for e in range(c):
+                    settle(s.land_r.at[layer, e], s.got_r.at[layer, e])
+                    s.send_p[layer, e, other] = (
+                        s.send_p[layer, e, other].astype(F32) + s.land_r[layer, e].astype(F32)
+                    ).astype(BF16)
+                    send_part(layer, e, other)
+                send_part(layer, c, other)
+                send_part(layer, c, across)
 
     def project(layer, rows):
         scale_row = s.gain[...].astype(F32)[layer : layer + 1]
@@ -220,21 +280,10 @@
                     preferred_element_type=F32,
                 )
                 put(s.send_p.at[layer, c], 0, acc)
-                if relay and c < 2 * blocks - 1:
+                if relay:
                     deal_relayed(layer, c)
                 else:
                     deal(s.send_p.at[layer, c], s.land_p.at[layer, c], "p", s.got_p.at[layer, c])
-        if relay:
-            @pl.when(inside)
-            def _():
-                end = (dp - 1) * 3
-                other = 3 - end
-                for c in range(2 * blocks - 1):
-                    settle(s.land_r.at[layer, c], s.got_r.at[layer, c])
-                    s.send_p[layer, c, other] = (
-                        s.send_p[layer, c, other].astype(F32) + s.land_r[layer, c].astype(F32)
-                    ).astype(BF16)
-                    send_part(layer, c, other)
 
     def total(mine, others):
         acc = mine[dp].astype(F32)
@@ -491,7 +540,7 @@
     "landed", "lhs_buf", "send_a", "land_a", "send_b", "land_b", "send_p", "land_p",
     "read", "drive_pad", "drive_t", "outer", "decay_pad", "decay_t",
     "held", "lhs_out", "parts", "rows", "send_f", "land_f", "land_r",
-    "small_sem", "weight_sem", "own_sem", "sent", "got_x", "got_a", "got_b", "got_p", "got_r",
+    "small_sem", "weight_sem", "own_sem", "know", "sent", "got_x", "got_a", "got_b", "got_p", "got_r",
     "got_n", "got_o", "got_f",
 )
 
@@ -536,7 +585,8 @@
         pltpu.VMEM((2, ntp, rows_t, width // 2), BF16),
         pltpu.VMEM((2, ntp, rows_t, width // 2), BF16),
         pltpu.VMEM((layers, chunks - 1, rows_d, block), BF16),
-        dma(len(SMALLS)), dma(layers, 7), dma(1), dma(len(SEND_KINDS)), dma(1), dma(layers),
+        dma(len(SMALLS)), dma(layers, 7), dma(1),
+        pltpu.SemaphoreType.REGULAR((2,)), dma(len(SEND_KINDS)), dma(1), dma(layers),
         dma(layers), dma(layers, chunks), dma(layers, chunks - 1), dma(layers, chunks // 2),
         dma(layers - 1, 2), dma(1, 2),
     ]

time: 52.7 us -> 48.8 us (0.926)
  Pallas kernels: 51.9 us -> 47.9 us
    pallas_call x1, Pallas kernels: 46 us -> 42 us  [shards(): pl.pallas_call(functools.partial(mixer_kernel, ntp, ndp, names), out_shap...]
where the time goes in v4:
time: 48.8 us; the launch traced here: 48.6 us
  Pallas kernels  47.9 us (98%)
  between operations  0.65 us (1%)
    pallas_call x1, Pallas kernels, shards(): pl.pallas_call(functools.partial(mixer_kernel, ntp, ndp, names), out_shap...  42 us
    pallas_call x1, Pallas kernels, shards(): pl.pallas_call(write_kernel, out_shape=tuple((jax.ShapeDtypeStruct(r.shap...  5.92 us

profile of v4, /device:TPU:0, one launch (start us, length us, event | category | flops | bytes accessed | tf_op | source)
XLA Modules:
  0.0 48.6 jit_solution(3306258802725572067)
XLA Ops:
  0.6 42.0 %shard_map.174 = (bf16[8,1024]{1,0:T(8,128)(2,1)S(1)}, bf16[2,3,8,2048]{3,2,1,0:T(8,128)(2,1)S(1)}, bf16[2,2,3,8,512]{4,3,2,1,0:T(8,128)(2,1)S(1)}, f32[2,8,32,64,128]{4,3,2,1,0:T(8,128)S(1)}) custom-call(bf16[8,1024]{1,0:T(8,128)(2,1)} %refs_0_.1, bf16[2,1024,128]{2,1,0:T(8,128)(2,1)} %refs_1_.1, bf16[2,2,1024,2048]{3,2,1,0:T(8,128)(2,1)} %refs_2_.1, ...), custom_call_target="tpu_custom_call" | custom-call | tf_op jit(solution)/shard_map/pallas_call | solution.py:600
  42.7 5.9 %shard_map.175 = (bf16[8,1024]{1,0:T(8,128)(2,1)}, bf16[2,3,8,2048]{3,2,1,0:T(8,128)(2,1)}, bf16[2,2,3,8,512]{4,3,2,1,0:T(8,128)(2,1)}, f32[2,8,32,64,128]{4,3,2,1,0:T(8,128)}) custom-call(bf16[8,1024]{1,0:T(8,128)(2,1)S(1)} %get-tuple-element.12.tok, bf16[2,3,8,2048]{3,2,1,0:T(8,128)(2,1)S(1)} %get-tuple-element.13.conv, ...), custom_call_target="tpu_custom_call" | custom-call | tf_op jit(solution)/shard_map/pallas_call | solution.py:610

commit v5 on v4

--- a/solution.py
+++ b/solution.py
@@ -52,7 +52,19 @@
     return barrier, ntp - 1 + jnp.asarray(dp > 0, jnp.int32) + jnp.asarray(dp < ndp - 1, jnp.int32)
 
 
-def pass_word(ndp, know):
+def learn_one(ndp, know):
+    dp = lax.axis_index("dp")
+
+    @pl.when(dp == 0)
+    def _():
+        pl.semaphore_wait(know.at[0], 1)
+
+    @pl.when(dp == ndp - 1)
+    def _():
+        pl.semaphore_wait(know.at[1], 1)
+
+
+def pass_word(ndp, know, ends):
     dp = lax.axis_index("dp")
 
     def tell(side, target):
@@ -66,6 +78,19 @@
         tell(1, dp + 1)
 
     for t in range(ndp - 2):
+        if not ends:
+            @pl.when(jnp.logical_and(dp > 0, dp < ndp - 2 - t))
+            def _():
+                pl.semaphore_wait(know.at[0], 1)
+                tell(0, dp - 1)
+
+            @pl.when(jnp.logical_and(dp > 1 + t, dp < ndp - 1))
+            def _():
+                pl.semaphore_wait(know.at[1], 1)
+                tell(1, dp + 1)
+
+            continue
+
         @pl.when(dp < ndp - 2 - t)
         def _():
             pl.semaphore_wait(know.at[0], 1)
@@ -147,27 +172,29 @@
 
     def load_weights(layer):
         vec = [
-            load(s.w_vec_hbm.at[layer, role], s.w_vec.at[layer, role], s.weight_sem.at[layer, role])
+            load(s.w_vec_hbm.at[layer, role], s.w_vec.at[layer, role], s.weight_sem.at[role])
             for role in (1, 0)
         ]
-        step = load(s.w_step_hbm.at[layer], s.w_step.at[layer], s.weight_sem.at[layer, 2])
+        step = load(s.w_step_hbm.at[layer], s.w_step.at[layer], s.weight_sem.at[2])
         return vec, step, [
-            load(s.w_in_hbm.at[layer, role], s.w_in.at[layer, role], s.weight_sem.at[layer, 3 + role])
+            load(s.w_in_hbm.at[layer, role], s.w_in.at[layer, role], s.weight_sem.at[3 + role])
             for role in (1, 0)
         ]
 
     def load_rest(layer):
         return (
-            load(s.ssm_hbm.at[layer], s.ssm.at[layer], s.weight_sem.at[layer, 5]),
-            load(s.w_out_hbm.at[layer], s.w_out.at[layer], s.weight_sem.at[layer, 6]),
+            load(s.ssm_hbm.at[layer], s.ssm.at[layer], s.rest_sem.at[layer, 0]),
+            load(s.w_out_hbm.at[layer], s.w_out.at[layer], s.rest_sem.at[layer, 1]),
         )
 
     barrier, callers = call_out(ntp, ndp)
-    load(s.x_hbm, s.landed.at[tp], s.own_sem.at[0]).wait()
+    own = load(s.x_hbm, s.landed.at[tp], s.own_sem.at[0])
+    smalls = [load(s.gain_hbm, s.gain, s.small_sem.at[0])]
+    own.wait()
     weights = [load_weights(0)]
-    smalls = [
+    smalls += [
         load(getattr(s, name + "_hbm"), getattr(s, name), s.small_sem.at[i])
-        for i, name in enumerate(SMALLS)
+        for i, name in enumerate(SMALLS) if i
     ]
     pl.semaphore_wait(barrier, callers)
     for k in range(1, ntp):
@@ -185,9 +212,8 @@
                 for c in range(2 * blocks - 1):
                     s.land_p[layer, c, across] = jnp.zeros((rows_d, block), BF16)
 
-    pass_word(ndp, s.know)
-    for copy in smalls:
-        copy.wait()
+    pass_word(ndp, s.know, not relay)
+    smalls[0].wait()
     settle(s.landed.at[pl.ds(0, ntp - 1)], s.got_x.at[0])
     rest = [load_rest(0)]
 
@@ -252,16 +278,32 @@
                     BF16
                 )
 
-        def deal(target, landing, kind, got):
-            for peer in far:
+        def deal(target, landing, kind, got, peers=far):
+            for peer in peers:
                 remote(
                     target.at[peer], landing.at[dp], s.sent.at[SEND_KINDS.index(kind)], got,
                     "dp", peer,
                 ).start()
 
+        def deal_small(kind, target, landing, got):
+            args = (target.at[layer], landing.at[layer], kind, got.at[layer])
+            if relay:
+                @pl.when(at_end)
+                def _():
+                    deal(*args, (middle,) if layer == 0 else (across, middle))
+
+                @pl.when(inside)
+                def _():
+                    deal(*args)
+            else:
+                deal(*args)
+            return args
+
         load_vec[0].wait()
         put(s.send_a.at[layer], 0, jnp.dot(lhs, s.w_vec[layer, 1], preferred_element_type=F32))
-        deal(s.send_a.at[layer], s.land_a.at[layer], "a", s.got_a.at[layer])
+        if relay and layer == 0:
+            learn_one(ndp, s.know)
+        late = [deal_small("a", s.send_a, s.land_a, s.got_a)]
         load_step.wait()
         load_vec[1].wait()
         small = jnp.dot(lhs, s.w_step[layer], preferred_element_type=F32)
@@ -270,7 +312,7 @@
         small = jnp.where(lane == local_heads, jnp.broadcast_to(squares, small.shape), small)
         put(s.send_b.at[layer], vcols, small)
         put(s.send_b.at[layer], 0, jnp.dot(lhs, s.w_vec[layer, 0], preferred_element_type=F32))
-        deal(s.send_b.at[layer], s.land_b.at[layer], "b", s.got_b.at[layer])
+        late.append(deal_small("b", s.send_b, s.land_b, s.got_b))
         for j, role in enumerate((1, 0)):
             load_in[j].wait()
             for b in range(blocks):
@@ -282,6 +324,20 @@
                 put(s.send_p.at[layer, c], 0, acc)
                 if relay:
                     deal_relayed(layer, c)
+                    if layer == 0 and c == blocks - 1:
+                        learn_one(ndp, s.know)
+
+                        @pl.when(at_end)
+                        def _():
+                            for args in late:
+                                deal(*args, (across,))
+
+                    if c == 2 * blocks - 2:
+                        @pl.when(at_end)
+                        def _():
+                            for args in late:
+                                deal(*args, (near,))
+
                 else:
                     deal(s.send_p.at[layer, c], s.land_p.at[layer, c], "p", s.got_p.at[layer, c])
 
@@ -307,6 +363,9 @@
             arrived(s.land_p.at[layer, c], s.got_p.at[layer, c])
 
     def head_step(layer):
+        if layer == 0:
+            for copy in smalls[1:]:
+                copy.wait()
         arrived(s.land_a.at[layer], s.got_a.at[layer])
         arrived(s.land_b.at[layer], s.got_b.at[layer])
         small = total(s.send_b.at[layer], s.land_b.at[layer])
@@ -385,8 +444,6 @@
                     + drive * inner[lane0 // span]
                     + expand(skips, head, rows_d) * v
                 )
-        for at in range(0, cols, LANES):
-            s.drive_t[at : at + LANES, :] = jnp.transpose(s.drive_pad[:, at : at + LANES])
         gain_row = s.out_gain[...].astype(F32)[layer : layer + 1]
         for b in range(blocks):
             c = blocks + b
@@ -400,14 +457,18 @@
                 s.held[layer, dp, :, cut] = (
                     part * lax.rsqrt(mean + EPS) * gain_row[:, cut]
                 ).astype(BF16)
-            mine = s.held.at[layer, dp, :, pl.ds(b * block, block)]
-            for peer in far:
-                remote(
-                    mine, mine, s.sent.at[SEND_KINDS.index("n")], s.got_n.at[layer, b], "dp", peer
-                ).start()
-
-    def update_state(layer):
+                g = (b * block + at) // span
+                mine = s.held.at[layer, dp, :, pl.ds(g * span, span)]
+                for peer in far:
+                    remote(
+                        mine, mine, s.sent.at[SEND_KINDS.index("n")], s.got_n.at[layer, g],
+                        "dp", peer,
+                    ).start()
+
+    def update_state(layer, half):
         some = min(4, group_heads)
+        for at in range(half * cols // 2, (half + 1) * cols // 2, LANES):
+            s.drive_t[at : at + LANES, :] = jnp.transpose(s.drive_pad[:, at : at + LANES])
 
         def some_heads(q, carry):
             first = q * some
@@ -427,15 +488,16 @@
                         )
             return carry
 
-        lax.fori_loop(0, local_heads // some, some_heads, 0)
+        steps = local_heads // some
+        lax.fori_loop(half * steps // 2, (half + 1) * steps // 2, some_heads, 0)
 
     def gather_out(layer, emit):
         rest[layer][1].wait()
         half = width // 2
         accs = [jnp.zeros((batch, half), F32)] * 2
-        for b in range(blocks):
-            cut = slice(b * block, (b + 1) * block)
-            settle(s.held.at[layer, pl.ds(0, ndp - 1), :, pl.ds(b * block, block)], s.got_n.at[layer, b])
+        for g in range(groups):
+            cut = slice(g * span, (g + 1) * span)
+            settle(s.held.at[layer, pl.ds(0, ndp - 1), :, pl.ds(g * span, span)], s.got_n.at[layer, g])
             for i in range(ndp):
                 s.lhs_out[i * rows_d : (i + 1) * rows_d, cut] = s.held[layer, i, :, cut].astype(F32)
             lhs = s.lhs_out[:, cut].astype(BF16)
@@ -443,7 +505,7 @@
                 accs[h] = accs[h] + jnp.dot(
                     lhs, s.w_out[layer, cut, h * half : (h + 1) * half], preferred_element_type=F32
                 )
-                if b == blocks - 1:
+                if g == groups - 1:
                     emit(h, accs[h])
 
     project(0, lambda i: s.landed[i].astype(F32))
@@ -453,7 +515,7 @@
             weights.append(load_weights(layer + 1))
             rest.append(load_rest(layer + 1))
         head_step(layer)
-        update_state(layer)
+        update_state(layer, 0)
         half = width // 2
 
         def emit(h, acc, layer=layer, last=last):
@@ -471,6 +533,7 @@
                 remote(src, dst, kind, got, "tp", peer).start()
 
         gather_out(layer, emit)
+        update_state(layer, 1)
         if last:
             for h in range(2):
                 cut = slice(h * half, (h + 1) * half)
@@ -540,7 +603,7 @@
     "landed", "lhs_buf", "send_a", "land_a", "send_b", "land_b", "send_p", "land_p",
     "read", "drive_pad", "drive_t", "outer", "decay_pad", "decay_t",
     "held", "lhs_out", "parts", "rows", "send_f", "land_f", "land_r",
-    "small_sem", "weight_sem", "own_sem", "know", "sent", "got_x", "got_a", "got_b", "got_p", "got_r",
+    "small_sem", "weight_sem", "rest_sem", "own_sem", "know", "sent", "got_x", "got_a", "got_b", "got_p", "got_r",
     "got_n", "got_o", "got_f",
 )
 
@@ -585,9 +648,9 @@
         pltpu.VMEM((2, ntp, rows_t, width // 2), BF16),
         pltpu.VMEM((2, ntp, rows_t, width // 2), BF16),
         pltpu.VMEM((layers, chunks - 1, rows_d, block), BF16),
-        dma(len(SMALLS)), dma(layers, 7), dma(1),
+        dma(len(SMALLS)), dma(5), dma(layers, 2), dma(1),
         pltpu.SemaphoreType.REGULAR((2,)), dma(len(SEND_KINDS)), dma(1), dma(layers),
-        dma(layers), dma(layers, chunks), dma(layers, chunks - 1), dma(layers, chunks // 2),
+        dma(layers), dma(layers, chunks), dma(layers, chunks - 1), dma(layers, groups),
         dma(layers - 1, 2), dma(1, 2),
     ]
     out_shape = (

time: 48.8 us -> 48 us (0.984)
  Pallas kernels: 47.9 us -> 47.2 us
    pallas_call x1, Pallas kernels: 42 us -> 41.2 us  [shards(): pl.pallas_call(functools.partial(mixer_kernel, ntp, ndp, names), out_shap...]
where the time goes in v5:
time: 48 us; the launch traced here: 47.8 us
  Pallas kernels  47.2 us (98%)
  between operations  0.65 us (1%)
    pallas_call x1, Pallas kernels, shards(): pl.pallas_call(functools.partial(mixer_kernel, ntp, ndp, names), out_shap...  41.2 us
    pallas_call x1, Pallas kernels, shards(): pl.pallas_call(write_kernel, out_shape=tuple((jax.ShapeDtypeStruct(r.shap...  5.92 us

profile of v5, /device:TPU:0, one launch (start us, length us, event | category | flops | bytes accessed | tf_op | source)
XLA Modules:
  0.0 47.8 jit_solution(4043177759882926731)
XLA Ops:
  0.6 41.2 %shard_map.174 = (bf16[8,1024]{1,0:T(8,128)(2,1)S(1)}, bf16[2,3,8,2048]{3,2,1,0:T(8,128)(2,1)S(1)}, bf16[2,2,3,8,512]{4,3,2,1,0:T(8,128)(2,1)S(1)}, f32[2,8,32,64,128]{4,3,2,1,0:T(8,128)S(1)}) custom-call(bf16[8,1024]{1,0:T(8,128)(2,1)} %refs_0_.1, bf16[2,1024,128]{2,1,0:T(8,128)(2,1)} %refs_1_.1, bf16[2,2,1024,2048]{3,2,1,0:T(8,128)(2,1)} %refs_2_.1, ...), custom_call_target="tpu_custom_call" | custom-call | tf_op jit(solution)/shard_map/pallas_call | solution.py:663
  41.9 5.9 %shard_map.175 = (bf16[8,1024]{1,0:T(8,128)(2,1)}, bf16[2,3,8,2048]{3,2,1,0:T(8,128)(2,1)}, bf16[2,2,3,8,512]{4,3,2,1,0:T(8,128)(2,1)}, f32[2,8,32,64,128]{4,3,2,1,0:T(8,128)}) custom-call(bf16[8,1024]{1,0:T(8,128)(2,1)S(1)} %get-tuple-element.12.tok, bf16[2,3,8,2048]{3,2,1,0:T(8,128)(2,1)S(1)} %get-tuple-element.13.conv, ...), custom_call_target="tpu_custom_call" | custom-call | tf_op jit(solution)/shard_map/pallas_call | solution.py:673

commit v6 on v5

--- a/solution.py
+++ b/solution.py
@@ -126,7 +126,7 @@
     return out
 
 
-SEND_KINDS = ("x", "a", "b", "p", "n", "o", "f")
+SEND_KINDS = ("x", "a", "b", "p", "n", "o", "f", "e", "q")
 
 
 def far_first(me, n):
@@ -159,6 +159,8 @@
     blocks = cols // block
     tp = lax.axis_index("tp")
     dp = lax.axis_index("dp")
+    core = lax.rem(tp, 2)
+    partner = tp + 1 - 2 * core
     far = far_first(dp, ndp)
     relay = ndp == 4
     at_end = jnp.logical_or(dp == 0, dp == ndp - 1)
@@ -520,36 +522,59 @@
 
         def emit(h, acc, layer=layer, last=last):
             kind = s.sent.at[SEND_KINDS.index("f" if last else "o")]
-            got = (s.got_f if last else s.got_o).at[0 if last else layer, h]
+            got = s.got_f.at[h] if last else s.got_o.at[layer]
             if last:
                 for i in range(ntp):
                     s.send_f[h, i] = acc[i * rows_t : (i + 1) * rows_t].astype(BF16)
+            elif h == 0:
+                s.parts[layer, tp] = acc.astype(BF16)
             else:
-                s.parts[layer, h, tp] = acc.astype(BF16)
+                for q in range(2):
+                    s.pair_out[layer, q] = acc[:, q * half // 2 : (q + 1) * half // 2].astype(BF16)
+                remote(
+                    s.pair_out.at[layer, 1 - core], s.pair_in.at[layer],
+                    s.sent.at[SEND_KINDS.index("e")], s.got_e.at[layer], "tp", partner,
+                ).start()
+                return
             for k in range(1, ntp):
                 peer = lax.rem(tp + k, ntp)
-                src = s.send_f.at[h, peer] if last else s.parts.at[layer, h, tp]
+                src = s.send_f.at[h, peer] if last else s.parts.at[layer, tp]
                 dst = s.land_f.at[h, tp] if last else src
                 remote(src, dst, kind, got, "tp", peer).start()
 
         gather_out(layer, emit)
+        if not last:
+            settle(s.pair_in.at[layer], s.got_e.at[layer])
+            s.quarters[layer, tp] = (
+                s.pair_out[layer, core].astype(F32) + s.pair_in[layer].astype(F32)
+            ).astype(BF16)
+            for k in range(1, ntp):
+                remote(
+                    s.quarters.at[layer, tp], s.quarters.at[layer, tp],
+                    s.sent.at[SEND_KINDS.index("q")], s.got_q.at[layer],
+                    "tp", lax.rem(tp + k, ntp),
+                ).start()
         update_state(layer, 1)
         if last:
             for h in range(2):
                 cut = slice(h * half, (h + 1) * half)
-                settle(s.land_f.at[h, pl.ds(0, ntp - 1)], s.got_f.at[0, h])
+                settle(s.land_f.at[h, pl.ds(0, ntp - 1)], s.got_f.at[h])
                 s.land_f[h, tp] = s.send_f[h, tp]
                 acc = s.rows[tp, :, cut].astype(F32)
                 for i in range(ntp):
                     acc = acc + s.land_f[h, i].astype(F32)
                 s.tokens[:, cut] = acc.astype(BF16)
         else:
-            accs = []
-            for h in range(2):
-                settle(s.parts.at[layer, h, pl.ds(0, ntp - 1)], s.got_o.at[layer, h])
-                acc = s.parts[layer, h, 0].astype(F32)
-                for i in range(1, ntp):
-                    acc = acc + s.parts[layer, h, i].astype(F32)
+            settle(s.parts.at[layer, pl.ds(0, ntp - 1)], s.got_o.at[layer])
+            acc = s.parts[layer, 0].astype(F32)
+            for i in range(1, ntp):
+                acc = acc + s.parts[layer, i].astype(F32)
+            accs = [acc]
+            settle(s.quarters.at[layer, pl.ds(0, ntp - 1)], s.got_q.at[layer])
+            for q in range(2):
+                acc = s.quarters[layer, q].astype(F32)
+                for i in range(q + 2, ntp, 2):
+                    acc = acc + s.quarters[layer, i].astype(F32)
                 accs.append(acc)
             acc = jnp.concatenate(accs, axis=1)
             before = s.landed if layer == 0 else s.rows
@@ -565,7 +590,9 @@
     settle(s.send_b.at[:, pl.ds(0, ndp - 1)], s.sent.at[2])
     settle(s.send_p.at[:, :, pl.ds(0, ndp - 1)], s.sent.at[3])
     settle(s.held.at[:, pl.ds(0, ndp - 1)], s.sent.at[4])
-    settle(s.parts.at[:, :, pl.ds(0, ntp - 1)], s.sent.at[5])
+    settle(s.parts.at[:, pl.ds(0, ntp - 1)], s.sent.at[5])
+    settle(s.pair_in, s.sent.at[7])
+    settle(s.quarters.at[:, pl.ds(0, ntp - 1)], s.sent.at[8])
     settle(s.land_f.at[:, pl.ds(0, ntp - 1)], s.sent.at[6])
 
 
@@ -602,9 +629,9 @@
 ) + SMALLS + (
     "landed", "lhs_buf", "send_a", "land_a", "send_b", "land_b", "send_p", "land_p",
     "read", "drive_pad", "drive_t", "outer", "decay_pad", "decay_t",
-    "held", "lhs_out", "parts", "rows", "send_f", "land_f", "land_r",
+    "held", "lhs_out", "parts", "pair_out", "pair_in", "quarters", "rows", "send_f", "land_f", "land_r",
     "small_sem", "weight_sem", "rest_sem", "own_sem", "know", "sent", "got_x", "got_a", "got_b", "got_p", "got_r",
-    "got_n", "got_o", "got_f",
+    "got_n", "got_o", "got_f", "got_e", "got_q",
 )
 
 
@@ -643,7 +670,10 @@
         pltpu.VMEM((LANES, LANES), F32),
         pltpu.VMEM((layers, ndp, rows_d, cols), BF16),
         pltpu.VMEM((batch, cols), F32),
-        pltpu.VMEM((layers - 1, 2, ntp, batch, width // 2), BF16),
+        pltpu.VMEM((layers - 1, ntp, batch, width // 2), BF16),
+        pltpu.VMEM((layers - 1, 2, batch, width // 4), BF16),
+        pltpu.VMEM((layers - 1, batch, width // 4), BF16),
+        pltpu.VMEM((layers - 1, ntp, batch, width // 4), BF16),
         pltpu.VMEM((ntp, rows_t, width), BF16),
         pltpu.VMEM((2, ntp, rows_t, width // 2), BF16),
         pltpu.VMEM((2, ntp, rows_t, width // 2), BF16),
@@ -651,7 +681,7 @@
         dma(len(SMALLS)), dma(5), dma(layers, 2), dma(1),
         pltpu.SemaphoreType.REGULAR((2,)), dma(len(SEND_KINDS)), dma(1), dma(layers),
         dma(layers), dma(layers, chunks), dma(layers, chunks - 1), dma(layers, groups),
-        dma(layers - 1, 2), dma(1, 2),
+        dma(layers - 1), dma(2), dma(layers - 1), dma(layers - 1),
     ]
     out_shape = (
         pltpu.VMEM(tokens.shape, BF16),

time: 48 us -> 48.1 us (level)
  no operation moved by 1% of the time
where the time goes in v6:
time: 48.1 us; the launch traced here: 47.8 us
  Pallas kernels  47.2 us (98%)
  between operations  0.65 us (1%)
    pallas_call x1, Pallas kernels, shards(): pl.pallas_call(functools.partial(mixer_kernel, ntp, ndp, names), out_shap...  41.3 us
    pallas_call x1, Pallas kernels, shards(): pl.pallas_call(write_kernel, out_shape=tuple((jax.ShapeDtypeStruct(r.shap...  5.92 us

profile of v6, /device:TPU:0, one launch (start us, length us, event | category | flops | bytes accessed | tf_op | source)
XLA Modules:
  0.0 47.8 jit_solution(10822011443947245909)
XLA Ops:
  0.6 41.3 %shard_map.174 = (bf16[8,1024]{1,0:T(8,128)(2,1)S(1)}, bf16[2,3,8,2048]{3,2,1,0:T(8,128)(2,1)S(1)}, bf16[2,2,3,8,512]{4,3,2,1,0:T(8,128)(2,1)S(1)}, f32[2,8,32,64,128]{4,3,2,1,0:T(8,128)S(1)}) custom-call(bf16[8,1024]{1,0:T(8,128)(2,1)} %refs_0_.1, bf16[2,1024,128]{2,1,0:T(8,128)(2,1)} %refs_1_.1, bf16[2,2,1024,2048]{3,2,1,0:T(8,128)(2,1)} %refs_2_.1, ...), custom_call_target="tpu_custom_call" | custom-call | tf_op jit(solution)/shard_map/pallas_call | solution.py:693
  41.9 5.9 %shard_map.175 = (bf16[8,1024]{1,0:T(8,128)(2,1)}, bf16[2,3,8,2048]{3,2,1,0:T(8,128)(2,1)}, bf16[2,2,3,8,512]{4,3,2,1,0:T(8,128)(2,1)}, f32[2,8,32,64,128]{4,3,2,1,0:T(8,128)}) custom-call(bf16[8,1024]{1,0:T(8,128)(2,1)S(1)} %get-tuple-element.12.tok, bf16[2,3,8,2048]{3,2,1,0:T(8,128)(2,1)S(1)} %get-tuple-element.13.conv, ...), custom_call_target="tpu_custom_call" | custom-call | tf_op jit(solution)/shard_map/pallas_call | solution.py:703
